TPU v7x, 32 devices: a whole 2x2x4 slice. The times are simulated.
32 devices in a mesh: grp: 2 (over y), sp: 4 (over z), tp: 4 (over x, core).
Axes of the slice: x: 2, y: 2, z: 4, core: 2. Of those that a mesh axis runs over, the one named last changes fastest.
Arguments:
- carryover_vector: bfloat16 [2048, 2048], P(('grp', 'sp', 'tp')), parts along dimension 0, may hold values from -6 to 6
- channel_source_entries: bfloat16 [2048, 1024], P(('grp', 'sp'), 'tp'), parts along dimension 0, may hold values from -6 to 6
- final_modulation_vector: bfloat16 [2048, 1024], P(('grp', 'sp'), 'tp'), parts along dimension 0, may hold values from -54 to 54
- entering_basis_matrix: bfloat16 [2048, 512], P(('grp', 'sp'), 'tp'), parts along dimension 0, may hold values from -6 to 6
- readout_basis_matrix: bfloat16 [2048, 512], P(('grp', 'sp'), 'tp'), parts along dimension 0, may hold values from -6 to 6
- raw_stride_amount: float32 [2048, 16], P(('grp', 'sp'), 'tp'), parts along dimension 0, may hold values from -6 to 5
- extra_log_attenuation: float32 [2048, 16], P(('grp', 'sp'), 'tp'), parts along dimension 0, may hold values from -1.4 to 0
- channel_fading_rate: float32 [16], P('tp'), may hold values from 0 to 0.1, as said below
- channel_source_kernel: float32 [4, 1024], P(None, 'tp'), may hold values from -3 to 3
- entering_basis_kernel: float32 [4, 512], P(None, 'tp'), may hold values from -3 to 3
- readout_basis_kernel: float32 [4, 512], P(None, 'tp'), may hold values from -3 to 3
- modulated_rescaling_vector: float32 [1024], replicated, may hold values from 0.1 to 1.9
- blender_final_matrix: bfloat16 [1024, 2048], replicated, may hold values from -0.1875 to 0.1875
- specialist_rescaling_vector: float32 [2048], replicated, may hold values from 0.1 to 1.9
- specialist_gating_matrices: bfloat16 [8, 2048, 1024], P('sp', None, 'tp'), may hold values from -0.125 to 0.125
- widening_matrices: bfloat16 [8, 2048, 1024], P('sp', None, 'tp'), may hold values from -0.125 to 0.125
- contracting_matrices: bfloat16 [8, 1024, 2048], P('sp', 'tp'), may hold values from -0.1875 to 0.1875
- assigned_specialist_ids: int32 [2048, 2], P(('grp', 'sp')), parts along dimension 0, may hold values from 0 to 7, as said below
- specialist_choice_affinity: float32 [2048, 2], P(('grp', 'sp', 'tp')), parts along dimension 0, may hold values from -6 to 6
- cluster_chance: float32 [2048], P(('grp', 'sp', 'tp')), parts along dimension 0, may hold values from 0.25 to 1
Outputs:
- layer_out: bfloat16 [2048, 2048], P(('grp', 'sp', 'tp')), parts along dimension 0
There are 2 independent parts, one for each index of `grp`. A program takes and returns all parts, laid end to end along the dimension named above; an argument that names none is the same for every part. Nothing has to cross between parts.
Inputs may be any that keep to these rules, and one draw needn't show every extreme that they name: `assigned_specialist_ids`: each row names 2 different experts of one group: the experts g * 2 to (g + 1) * 2 - 1 for one g below 4. In each aligned block of 64 rows (the rows of one device) no expert is named by more than 32 rows, and every expert of one group, the same group in all blocks, is named by exactly 32 rows of every block. `channel_fading_rate`: positive.
All inputs are finite; a program needn't handle non-finite values.
Results may differ from a plain program's by a relative error of at most 0.015.
Values may be sent and summed in bfloat16 or wider, within the bound.
No kernel may reach another device: no remote copies, remote signals or barrier semaphores. Data moves between devices by JAX's collectives and lax.ppermute only.
A program may use at most 64 MiB of HBM per device.

v0:
```python
import jax
import jax.numpy as jnp
from jax import lax
from jax.sharding import PartitionSpec as P

HEAD_DIM = 64
STATE = 128
BLOCK = 64


EPS = 1e-06
HIGHEST = lax.Precision.HIGHEST


def prefix(x, axis, combine, identity):
    size, index = (lax.axis_size(axis), lax.axis_index(axis))
    everything = jax.tree.map(
        lambda part, kind: lax.all_gather(part.astype(kind), axis), x, (jnp.bfloat16, jnp.bfloat16)
    )
    start = jax.tree.map(
        lambda part, zero: jnp.broadcast_to(jnp.asarray(zero, part.dtype), part.shape), x, identity
    )

    def lap(k, before):
        reached = k < index
        new = combine(
            before, jax.tree.map(lambda part, own: part[k].astype(own.dtype), everything, x)
        )
        return jax.tree.map(lambda a, b: jnp.where(reached, a, b), new, before)

    return lax.fori_loop(0, size, lap, start)


def from_behind(x, axis, by):
    size = lax.axis_size(axis)
    pairs = [(i, i + by) for i in range(size) if 0 <= i + by < size]
    return lax.ppermute(x, axis, pairs)


def causal_conv(signal, earlier, weights):
    kernel_len = weights.shape[0]
    length = signal.shape[0]
    joined = jnp.concatenate([earlier, signal], axis=0).astype(jnp.float32)
    accumulated = jnp.zeros((length, signal.shape[1]), jnp.float32)
    for offset in range(kernel_len):
        accumulated = accumulated + weights[offset][None, :] * joined[offset : offset + length]
    return jax.nn.silu(accumulated)


def link_states(earlier, later):
    return (earlier[0] * later[0], earlier[1] * later[0][..., None, None] + later[1])


def device_states(scaled_in, log_attenuation, keys_b, queries_c, groups_here):
    length = scaled_in.shape[0]
    blocks = length // BLOCK
    per_group = scaled_in.shape[1] // groups_here
    scaled_in = scaled_in.reshape(blocks, BLOCK, groups_here, per_group, HEAD_DIM)
    log_attenuation = log_attenuation.reshape(blocks, BLOCK, groups_here, per_group)
    keys_b = keys_b.reshape(blocks, BLOCK, groups_here, STATE)
    queries_c = queries_c.reshape(blocks, BLOCK, groups_here, STATE)
    running = jnp.cumsum(log_attenuation, axis=1)
    lower_mask = jnp.tril(jnp.ones((BLOCK, BLOCK), dtype=bool))
    between = running[:, :, None] - running[:, None, :]
    decays = jnp.exp(jnp.where(lower_mask[None, :, :, None, None], between, -jnp.inf))
    scores = jnp.einsum("blgn,bsgn->blsg", queries_c, keys_b, precision=HIGHEST)
    inside = jnp.einsum("blsg,blsgr,bsgrp->blgrp", scores, decays, scaled_in, precision=HIGHEST)
    totals = running[:, -1]
    remain = jnp.exp(totals[:, None] - running)
    block_states = jnp.einsum(
        "bsgn,bsgr,bsgrp->bgrpn", keys_b, remain, scaled_in, precision=HIGHEST
    )

    def advance(carried, pieces):
        return (carried * jnp.exp(pieces[1])[..., None, None] + pieces[0], carried)

    initial = jnp.zeros(block_states.shape[1:], jnp.float32)
    own_state, entering = lax.scan(advance, initial, (block_states, totals))
    own_decay = jnp.exp(jnp.sum(totals, axis=0))
    _, incoming = prefix(
        (own_decay, own_state),
        "sp",
        link_states,
        (jnp.ones_like(own_decay), jnp.zeros_like(own_state)),
    )
    preceding = jnp.exp(jnp.cumsum(totals, axis=0) - totals)
    entering = entering + preceding[..., None, None] * incoming[None]
    outside = jnp.einsum(
        "blgn,bgrpn,blgr->blgrp", queries_c, entering, jnp.exp(running), precision=HIGHEST
    )
    return (inside + outside).reshape(length, -1)


def fetch_rows(tokens, sources):
    present = sources >= 0
    picked = jnp.take(tokens, jnp.maximum(sources, 0), axis=0)
    return jnp.where(present[:, None], picked, jnp.zeros_like(picked))


def slot_tables(chosen_ids, quarters, row_count, experts, capacity):
    picks = chosen_ids.shape[1]
    flat_ids = chosen_ids.reshape(quarters, row_count * picks)
    member = (flat_ids[..., None] == jnp.arange(experts, dtype=jnp.int32)).astype(jnp.int32)
    position = jnp.sum((jnp.cumsum(member, axis=1) - member) * member, axis=2)
    quarter_ids = jnp.arange(quarters, dtype=jnp.int32)[:, None]
    slot_index = flat_ids * (quarters * capacity) + quarter_ids * capacity + position
    token_index = (
        quarter_ids * row_count + jnp.arange(row_count * picks, dtype=jnp.int32)[None, :] // picks
    )
    sources = (
        jnp.full((experts * quarters * capacity,), -1, jnp.int32)
        .at[slot_index.reshape(-1)]
        .set(token_index.reshape(-1))
    )
    return (sources, position)


def per_device(
    carryover_vector,
    channel_source_entries,
    final_modulation_vector,
    entering_basis_matrix,
    readout_basis_matrix,
    raw_stride_amount,
    extra_log_attenuation,
    channel_fading_rate,
    channel_source_kernel,
    entering_basis_kernel,
    readout_basis_kernel,
    modulated_rescaling_vector,
    blender_final_matrix,
    specialist_rescaling_vector,
    specialist_gating_matrices,
    widening_matrices,
    contracting_matrices,
    assigned_specialist_ids,
    specialist_choice_affinity,
    cluster_chance,
):
    length = channel_source_entries.shape[0]
    row_count = carryover_vector.shape[0]
    model_width = carryover_vector.shape[1]
    heads_here = channel_fading_rate.shape[0]
    groups_here = entering_basis_matrix.shape[1] // STATE
    tp_index = lax.axis_index("tp")
    rim_rows = channel_source_kernel.shape[0] - 1
    neighbours = from_behind(
        (
            channel_source_entries[length - rim_rows :],
            entering_basis_matrix[length - rim_rows :],
            readout_basis_matrix[length - rim_rows :],
        ),
        "sp",
        1,
    )
    inputs_x = causal_conv(channel_source_entries, neighbours[0], channel_source_kernel)
    keys_b = causal_conv(entering_basis_matrix, neighbours[1], entering_basis_kernel)
    queries_c = causal_conv(readout_basis_matrix, neighbours[2], readout_basis_kernel)
    channel_stride_amount = jax.nn.softplus(raw_stride_amount)
    log_attenuation = extra_log_attenuation - channel_fading_rate[None, :] * channel_stride_amount
    heads_x = inputs_x.reshape(length, heads_here, HEAD_DIM)
    mixed = device_states(
        heads_x * channel_stride_amount[:, :, None], log_attenuation, keys_b, queries_c, groups_here
    )
    gated = mixed * jax.nn.silu(final_modulation_vector.astype(jnp.float32))
    head_cols = gated.shape[1]
    squares = lax.psum(jnp.sum(gated * gated, axis=1), "tp")
    first_col = tp_index * head_cols
    gain_part = lax.dynamic_slice_in_dim(modulated_rescaling_vector, first_col, head_cols, 0)
    scale = lax.rsqrt(squares / (head_cols * lax.axis_size("tp")) + EPS)
    normed = (gated * scale[:, None] * gain_part[None, :]).astype(jnp.bfloat16)
    weight_rows = lax.dynamic_slice_in_dim(blender_final_matrix, first_col, head_cols, 0)
    summed = lax.psum_scatter(
        jnp.dot(normed, weight_rows, preferred_element_type=jnp.float32).astype(jnp.bfloat16),
        "tp",
        scatter_dimension=0,
        tiled=True,
    ).astype(jnp.float32)
    middle = (carryover_vector.astype(jnp.float32) + summed).astype(jnp.bfloat16)
    middle_wide = middle.astype(jnp.float32)
    expert_input = (
        middle_wide
        * lax.rsqrt(jnp.mean(middle_wide * middle_wide, axis=1, keepdims=True) + EPS)
        * specialist_rescaling_vector[None, :]
    ).astype(jnp.bfloat16)
    sp_count = lax.axis_size("sp")
    local_experts = specialist_gating_matrices.shape[0]
    experts = sp_count * local_experts
    picks = assigned_specialist_ids.shape[1]
    capacity = 2 * row_count * picks // experts
    own_ids = lax.dynamic_slice_in_dim(assigned_specialist_ids, tp_index * row_count, row_count, 0)
    sources, position = slot_tables(own_ids, 1, row_count, experts, capacity)
    own_position = position[0]
    outgoing = fetch_rows(expert_input, sources).reshape(
        sp_count, local_experts, 1, capacity, model_width
    )
    received = lax.all_to_all(outgoing, "sp", split_axis=0, concat_axis=0, tiled=True)
    arrived = lax.all_gather(received, "tp", axis=2, tiled=True)
    gate_value = jnp.einsum(
        "slqcd,ldf->slqcf", arrived, specialist_gating_matrices, preferred_element_type=jnp.float32
    )
    up_value = jnp.einsum(
        "slqcd,ldf->slqcf", arrived, widening_matrices, preferred_element_type=jnp.float32
    )
    hidden = (jax.nn.silu(gate_value) * up_value).astype(jnp.bfloat16)
    partial_value = jnp.einsum(
        "slqcf,lfd->slqcd", hidden, contracting_matrices, preferred_element_type=jnp.float32
    )
    width_total = lax.psum_scatter(
        partial_value.astype(jnp.bfloat16), "tp", scatter_dimension=2, tiled=True
    )
    returned = lax.all_to_all(width_total, "sp", split_axis=0, concat_axis=0, tiled=True)
    answers = returned.reshape(experts * capacity, model_width)
    own_slots = own_ids.reshape(-1) * capacity + own_position
    gathered = (
        jnp.take(answers, own_slots, axis=0)
        .reshape(row_count, picks, model_width)
        .astype(jnp.float32)
    )
    lifted = jnp.exp(specialist_choice_affinity)
    shares = cluster_chance[:, None] * lifted / jnp.sum(lifted, axis=1, keepdims=True)
    return (middle_wide + jnp.sum(shares[:, :, None] * gathered, axis=1)).astype(jnp.bfloat16)


def solution(mesh):
    return jax.shard_map(
        per_device,
        mesh=mesh,
        in_specs=(
            P(("grp", "sp", "tp"), None),
            P(("grp", "sp"), "tp"),
            P(("grp", "sp"), "tp"),
            P(("grp", "sp"), "tp"),
            P(("grp", "sp"), "tp"),
            P(("grp", "sp"), "tp"),
            P(("grp", "sp"), "tp"),
            P("tp"),
            P(None, "tp"),
            P(None, "tp"),
            P(None, "tp"),
            P(),
            P(),
            P(),
            P("sp", None, "tp"),
            P("sp", None, "tp"),
            P("sp", "tp", None),
            P(("grp", "sp"), None),
            P(("grp", "sp", "tp"), None),
            P(("grp", "sp", "tp")),
        ),
        out_specs=P(("grp", "sp", "tp"), None),
        check_vma=False,
    )
```

profile of v0, /device:TPU:0, one launch (start us, length us, event | category | flops | bytes accessed | tf_op | source)
XLA Modules:
  0.0 319.8 jit_solution(16256433366509483427)
XLA Ops:
  6.5 0.8 slice.103
  7.4 4.9 %collective-permute-start.2 = (bf16[3,256]{1,0:T(4,128)(2,1)S(1)}, bf16[3,256]{1,0:T(4,128)(2,1)S(1)}, u32[]{:S(2)}, u32[]{:S(2)}) collective-permute-start(bf16[3,256]{1,0:T(4,128)(2,1)S(1)} %slice.103), channel_id=1, source_target_pairs={{0,4},{4,8},{8,12},{1,5},{5,9},{9,13},{2,6},{6,10},{10,14},{3,7},{... | collective-permute-start | bytes 4616 | tf_op jit(solution)/shard_map/ppermute | solution.py:37
  12.3 0.7 slice.85
  13.0 3.5 %collective-permute-start = (bf16[3,128]{1,0:T(4,128)(2,1)S(1)}, bf16[3,128]{1,0:T(4,128)(2,1)S(1)}, u32[]{:S(2)}, u32[]{:S(2)}) collective-permute-start(bf16[3,128]{1,0:T(4,128)(2,1)S(1)} %slice.85), channel_id=1, source_target_pairs={{0,4},{4,8},{8,12},{1,5},{5,9},{9,13},{2,6},{6,10},{10,14},{3,7},{... | collective-permute-start | bytes 2312 | tf_op jit(solution)/shard_map/ppermute | solution.py:37
  16.5 0.7 slice.94
  17.2 3.5 %collective-permute-start.1 = (bf16[3,128]{1,0:T(4,128)(2,1)S(1)}, bf16[3,128]{1,0:T(4,128)(2,1)S(1)}, u32[]{:S(2)}, u32[]{:S(2)}) collective-permute-start(bf16[3,128]{1,0:T(4,128)(2,1)S(1)} %slice.94), channel_id=1, source_target_pairs={{0,4},{4,8},{8,12},{1,5},{5,9},{9,13},{2,6},{6,10},{10,14},{3,7},{... | collective-permute-start | bytes 2312 | tf_op jit(solution)/shard_map/ppermute | solution.py:37
  20.7 0.6 iota_compare_fusion.1
  21.3 0.8 fusion.74
  22.1 0.8 slice_bitcast_fusion.7
  23.0 0.8 compare_select_fusion
  24.0 0.6 slice_reduce_fusion
  24.7 0.7 copy.81
  25.5 1.2 dynamic-slice
  27.7 8.4 %all-reduce = bf16[16]{0:T(256)(128)(2,1)S(1)} all-reduce(bf16[16]{0:T(256)(128)(2,1)S(1)} %dynamic-update-slice), channel_id=2, replica_groups=mesh['grp'=2,'sp'=4,'tp'=4] {'sp'}, use_global_device_ids=true, to_apply=%add | all-reduce | flops 16 | bytes 64
  36.0 0.7 reshape.446
  36.7 0.8 slice_bitcast_fusion.3
  37.6 0.6 subtract_exponential_fusion.1
  38.1 0.7 copy.80
  38.8 1.3 dynamic_slice.31
  40.2 0.9 maximum_convert_fusion.1
  41.2 0.9 maximum_convert_fusion.2
  42.5 0.8 copy.73
  43.3 0.9 maximum_convert_fusion
  44.8 1.5 convolution_bitcast_fusion
  46.4 5.6 %while.27 = (s32[]{:T(128)}, f32[1,4,64,128]{3,2,1,0:T(8,128)S(1)}, f32[4,1,4,64,128]{4,3,2,1,0:T(8,128)}, f32[4,1,4]{2,1,0:T(1,128)}, f32[4,1,4,64,128]{4,3,2,1,0:T(8,128)S(1)}, /*index=5*/s32[]{:T(128)}, s32[]{:T(128)}) while((s32[]{:T(128)}, f32[1,4,64,128]{3,2,1,0:T(8,128)S(1)}, f32[4,1,4,64,128]{4,3,2,1,0:T(8,128)}, ...), condition=%wide.region_2.3_spmd.clone, body=%wide.region_1.2_spmd.clone.sunk | while | flops 131075 | bytes 656016 | solution.py:78
  46.4 0.7 bitcast_dynamic-update-slice_fusion.2
  47.1 0.6 fusion.85
  47.8 0.7 bitcast_dynamic-update-slice_fusion.2
  48.4 0.7 fusion.85
  49.2 0.7 bitcast_dynamic-update-slice_fusion.2
  49.9 0.6 fusion.85
  50.6 0.7 bitcast_dynamic-update-slice_fusion.2
  51.3 0.6 fusion.85
  52.0 13.9 %all-gather.1 = bf16[4,4,64,128]{3,2,1,0:T(8,128)(2,1)S(1)} all-gather(bf16[1,4,64,128]{3,2,1,0:T(8,128)(2,1)S(1)} %convert_element_type.121), channel_id=3, replica_groups=mesh['grp'=2,'sp'=4,'tp'=4] {'sp'}, dimensions={0}, use_global_device_ids=true | all-gather | bytes 327680 | tf_op jit(solution)/shard_map/all_gather | solution.py:18
  66.0 3.0 while.28
  66.0 0.6 bitcast_convert_fusion.2
  66.7 0.6 bitcast_convert_fusion.2
  67.5 0.6 bitcast_convert_fusion.2
  68.2 0.7 bitcast_convert_fusion.2
  68.9 2.8 fusion.20
  71.7 2.0 fusion.21
  74.6 5.7 %psum.7 = f32[256]{0:T(256)S(1)} all-reduce(f32[256]{0:T(256)S(1)} %multiply_reduce_fusion.1), channel_id=1, replica_groups=mesh['grp'=2,'sp'=4,'tp'=4] {'tp'}, use_global_device_ids=true, to_apply=%region_8.9 | all-reduce | flops 256 | bytes 2048 | tf_op jit(solution)/shard_map/psum | solution.py:167
  80.3 2.7 convolution_convert_fusion
  84.1 1.0 scatter_custom_fusion
  85.3 22.6 %reduce-scatter.5.cloned.1.call-done = bf16[64,2048]{1,0:T(8,128)(2,1)} async-done(((bf16[256,2048]{1,0:T(8,128)(2,1)}), bf16[64,2048]{1,0:T(8,128)(2,1)}) %reduce-scatter.5.cloned.1.call-update) | async-done | bytes 262160 | tf_op jit(solution)/shard_map/reduce_scatter | solution.py:173
  108.0 1.1 fusion.25
  109.1 1.1 fusion.27
  110.2 1.4 gather_fusion
  111.8 30.0 %all_to_all.10 = bf16[4,2,1,32,2048]{4,3,2,1,0:T(8,128)(2,1)S(1)} all-to-all(bf16[4,2,1,32,2048]{4,3,2,1,0:T(8,128)(2,1)S(1)} %select_bitcast_fusion), channel_id=1, replica_groups=mesh['grp'=2,'sp'=4,'tp'=4] {'sp'}, dimensions={0} | all-to-all | bytes 2097152 | tf_op jit(solution)/shard_map/all_to_all | solution.py:197
  141.8 1.0 copy.93
  143.1 32.5 %all-gather.4.cloned.1.call-done = bf16[4,2,4,32,2048]{4,3,2,0,1:T(8,128)(2,1)} async-done(((bf16[4,2,1,32,2048]{4,3,2,0,1:T(8,128)(2,1)}), bf16[4,2,4,32,2048]{4,3,2,0,1:T(8,128)(2,1)}) %all-gather.4.cloned.1.call-update) | async-done | bytes 4194320 | tf_op jit(solution)/shard_map/all_gather | solution.py:198
  175.6 4.1 %fusion.8 = f32[4,2,4,32,256]{4,3,2,0,1:T(8,128)S(1)} fusion(bf16[4,2,4,32,2048]{4,3,2,0,1:T(8,128)(2,1)} %all-gather.4.cloned.1.call-done, bf16[2,2048,256]{2,1,0:T(8,128)(2,1)} %param.38), kind=kOutput, calls=%fused_computation.18 | convolution fusion | flops 1073741824 | bytes 7340032 | tf_op jit(solution)/shard_map/slqcd,ldf->slqcf/dot_general | solution.py:199
  179.7 7.3 %convert_bitcast_fusion = bf16[4,2,4,32,2048]{4,3,2,0,1:T(8,128)(2,1)} fusion(bf16[2,256,2048]{2,1,0:T(8,128)(2,1)S(1)} %copy-done, bf16[4,2,4,32,2048]{4,3,2,0,1:T(8,128)(2,1)} %all-gather.4.cloned.1.call-done, bf16[2,2048,256]{2,1,0:T(8,128)(2,1)} %param.39, f32[4,2,4,32,256]{4,3,2,0,1:T(8,128)S(1)} %fusion.8), kind=kOutput, calls=%fused_computation.11 | convolution fusion | flops 2151153664 | bytes 13631488 | tf_op jit(solution)/shard_map/slqcf,lfd->slqcd/dot_general | solution.py:206
  187.1 0.6 copy-done.10
  187.7 0.6 dynamic-slice.1
  188.3 84.4 %all-reduce.4.cloned.1.call-done = bf16[4,2,4,32,2048]{4,3,2,0,1:T(8,128)(2,1)} async-done(((bf16[4,2,4,32,2048]{4,3,2,0,1:T(8,128)(2,1)}), bf16[4,2,4,32,2048]{4,3,2,0,1:T(8,128)(2,1)}) %all-reduce.4.cloned.1.call-update) | async-done | bytes 4194320
  272.7 1.9 constant_dynamic-slice_fusion.1
  274.6 1.1 copy.94
  275.7 4.7 %all-to-all-start.1 = ((bf16[4,2,1,32,2048]{4,3,2,1,0:T(8,128)(2,1)}), bf16[4,2,1,32,2048]{4,3,2,1,0:T(8,128)(2,1)S(1)}, u32[]{:S(2)}, u32[]{:S(2)}) async-start(bf16[4,2,1,32,2048]{4,3,2,1,0:T(8,128)(2,1)} %copy.94), calls=%async_computation.2 | async-start | bytes 2097152 | tf_op jit(solution)/shard_map/all_to_all | solution.py:212
  280.9 24.9 %all-to-all-done.1 = bf16[4,2,1,32,2048]{4,3,2,1,0:T(8,128)(2,1)S(1)} async-done(((bf16[4,2,1,32,2048]{4,3,2,1,0:T(8,128)(2,1)}), bf16[4,2,1,32,2048]{4,3,2,1,0:T(8,128)(2,1)S(1)}, u32[]{:S(2)}, u32[]{:S(2)}) %all-to-all-start.1) | async-done | bytes 1048608 | tf_op jit(solution)/shard_map/all_to_all | solution.py:212
  305.8 1.7 gather_fusion.1
  307.5 1.4 gather.15
  308.9 2.5 multiply_reduce_fusion
  311.5 1.8 fusion.28
  (87 shorter events, 5.7 us)
Async XLA Ops:
  6.5 173.2 %copy-start = (bf16[2,256,2048]{2,1,0:T(8,128)(2,1)S(1)}, bf16[2,256,2048]{2,1,0:T(8,128)(2,1)}, u32[]{:S(2)}) copy-start(bf16[2,256,2048]{2,1,0:T(8,128)(2,1)} %param.40) | copy-start | bytes 6291460
  6.5 101.4 %reduce-scatter.5.cloned.1.call-start = ((), (), s32[]{:S(2)}) async-start(), calls=%async_computation.3 | async-start | bytes 1310720 | tf_op jit(solution)/shard_map/reduce_scatter | solution.py:173
  7.4 35.9 %collective-permute-start.2 = (bf16[3,256]{1,0:T(4,128)(2,1)S(1)}, bf16[3,256]{1,0:T(4,128)(2,1)S(1)}, u32[]{:S(2)}, u32[]{:S(2)}) collective-permute-start(bf16[3,256]{1,0:T(4,128)(2,1)S(1)} %slice.103), channel_id=1, source_target_pairs={{0,4},{4,8},{8,12},{1,5},{5,9},{9,13},{2,6},{6,10},{10,14},{3,7},{... | collective-permute-start | bytes 4616 | tf_op jit(solution)/shard_map/ppermute | solution.py:37
  13.0 27.1 %collective-permute-start = (bf16[3,128]{1,0:T(4,128)(2,1)S(1)}, bf16[3,128]{1,0:T(4,128)(2,1)S(1)}, u32[]{:S(2)}, u32[]{:S(2)}) collective-permute-start(bf16[3,128]{1,0:T(4,128)(2,1)S(1)} %slice.85), channel_id=1, source_target_pairs={{0,4},{4,8},{8,12},{1,5},{5,9},{9,13},{2,6},{6,10},{10,14},{3,7},{... | collective-permute-start | bytes 2312 | tf_op jit(solution)/shard_map/ppermute | solution.py:37
  17.2 24.0 %collective-permute-start.1 = (bf16[3,128]{1,0:T(4,128)(2,1)S(1)}, bf16[3,128]{1,0:T(4,128)(2,1)S(1)}, u32[]{:S(2)}, u32[]{:S(2)}) collective-permute-start(bf16[3,128]{1,0:T(4,128)(2,1)S(1)} %slice.94), channel_id=1, source_target_pairs={{0,4},{4,8},{8,12},{1,5},{5,9},{9,13},{2,6},{6,10},{10,14},{3,7},{... | collective-permute-start | bytes 2312 | tf_op jit(solution)/shard_map/ppermute | solution.py:37
  41.1 1.0 copy-start.3
  52.0 22.5 %copy-start.4 = (bf16[256,256]{1,0:T(8,128)(2,1)S(1)}, bf16[256,256]{1,0:T(8,128)(2,1)}, u32[]{:S(2)}) copy-start(bf16[256,256]{1,0:T(8,128)(2,1)} %param.26) | copy-start | bytes 393220
  52.0 28.3 %copy-start.7 = (f32[256]{0:T(256)S(1)}, f32[256]{0:T(256)}, u32[]{:S(2)}) copy-start(f32[256]{0:T(256)} %dynamic_slice.31) | copy-start | bytes 3076
  68.9 14.2 %copy-start.8 = (s32[256,2]{0,1:T(2,128)S(1)}, s32[256,2]{0,1:T(2,128)}, u32[]{:S(2)}) copy-start(s32[256,2]{0,1:T(2,128)} %param.41) | copy-start | bytes 6148
  71.7 36.3 %copy-start.1 = (bf16[64,2048]{1,0:T(8,128)(2,1)S(1)}, bf16[64,2048]{1,0:T(8,128)(2,1)}, u32[]{:S(2)}) copy-start(bf16[64,2048]{1,0:T(8,128)(2,1)} %param.24) | copy-start | bytes 786436
  71.7 37.4 %copy-start.5 = (f32[2048]{0:T(1024)S(1)}, f32[2048]{0:T(1024)}, u32[]{:S(2)}) copy-start(f32[2048]{0:T(1024)} %param.37) | copy-start | bytes 24580
  83.1 92.5 %all-gather.4.cloned.1.call-start = ((), (), s32[]{:S(2)}) async-start(), calls=%async_computation.4 | async-start | bytes 5242880 | tf_op jit(solution)/shard_map/all_gather | solution.py:198
  142.8 129.8 %all-reduce.4.cloned.1.call-start = ((), (), s32[]{:S(2)}) async-start(), calls=%async_computation.5 | async-start | bytes 8388608
  187.0 0.7 copy-start.10
  187.0 93.7 %copy-start.6 = (f32[64,2]{0,1:T(2,128)S(1)}, f32[64,2]{0,1:T(2,128)}, u32[]{:S(2)}) copy-start(f32[64,2]{0,1:T(2,128)} %param.42) | copy-start | bytes 1540
  187.1 93.7 %copy-start.9 = (f32[64]{0:T(128)S(1)}, f32[64]{0:T(128)}, u32[]{:S(2)}) copy-start(f32[64]{0:T(128)} %param.43) | copy-start | bytes 772
  275.7 35.8 %copy-start.2 = (bf16[64,2048]{1,0:T(8,128)(2,1)S(1)}, bf16[64,2048]{1,0:T(8,128)(2,1)}, u32[]{:S(2)}) copy-start(bf16[64,2048]{1,0:T(8,128)(2,1)} %param.24) | copy-start | bytes 786436
  275.7 30.1 %all-to-all-start.1 = ((bf16[4,2,1,32,2048]{4,3,2,1,0:T(8,128)(2,1)}), bf16[4,2,1,32,2048]{4,3,2,1,0:T(8,128)(2,1)S(1)}, u32[]{:S(2)}, u32[]{:S(2)}) async-start(bf16[4,2,1,32,2048]{4,3,2,1,0:T(8,128)(2,1)} %copy.94), calls=%async_computation.2 | async-start | bytes 2097152 | tf_op jit(solution)/shard_map/all_to_all | solution.py:212
Sparse Core Ops, SparseCore 0:
  83.2 24.7 reduce-scatter.4
  143.0 32.5 all-gather.3
  187.2 85.4 all-reduce.3
where the time goes:
time: 321 us; the launch traced here: 320 us
  waiting for transfers between devices  165 us (51%)
  blocking collectives  57.9 us (18%)
  local copies, waits for them, and re-layouts  26.1 us (8%)
  matrix products  20.8 us (6%)
  other arithmetic  19.1 us (6%)
  starting transfers between devices  16.9 us (5%)
  between operations  14.2 us (4%)
    unnamed x4, waiting for transfers between devices  84.5 us
    all_gather x1, waiting for transfers between devices, per_device(): arrived = lax.all_gather(received, 'tp', axis=2, tiled=True)  32.5 us
    all_to_all x1, blocking collectives, per_device(): lax.all_to_all(outgoing, 'sp', split_axis=0, concat_axis=0, tiled=True)  30 us
    all_to_all x1, waiting for transfers between devices, per_device(): lax.all_to_all(width_total, 'sp', split_axis=0, concat_axis=0, tiled=True)  24.9 us
    reduce_scatter x1, waiting for transfers between devices, per_device(): lax.psum_scatter(jnp.dot(normed, weight_rows, preferred_element_type=jnp....  22.6 us
    all_gather x1, blocking collectives, prefix(): lax.all_gather(part.astype(kind), axis)  13.9 us
    ppermute x3, starting transfers between devices, from_behind(): return lax.ppermute(x, axis, pairs)  11.9 us
    unnamed x1, blocking collectives  8.36 us
  transfers between devices with their start and end apart: 7, of which 4 were waited for; matrix products, arithmetic and copies ran while one was open for 6% of the time, Pallas kernels for 0%

commit v1 on v0

v1 whole, which is shorter than its diff:
```python
import jax
import jax.numpy as jnp
from jax import lax
from jax.sharding import PartitionSpec as P

HEAD_DIM = 64
STATE = 128
BLOCK = 64
EGROUPS = 4
MANY = 8


EPS = 1e-06
HIGHEST = lax.Precision.HIGHEST


def shifted(x, axis, by):
    size = lax.axis_size(axis)
    return lax.ppermute(x, axis, [(i, (i + by) % size) for i in range(size)])


def flipped(x, axis, bit):
    return lax.ppermute(x, axis, [(i, i ^ bit) for i in range(lax.axis_size(axis))])


def incoming_states(own_state, own_decay):
    size, index = (lax.axis_size("sp"), lax.axis_index("sp"))
    groups, per_group, width, entries = own_state.shape
    heads = groups * per_group
    rows = heads * width
    extra = -(-heads // 16) * 16
    decay_rows = jnp.broadcast_to(own_decay.reshape(heads, 1), (heads, entries))
    packed = jnp.concatenate(
        [
            own_state.reshape(rows, entries).astype(jnp.bfloat16),
            jnp.pad(decay_rows, ((0, extra - heads), (0, 0))).astype(jnp.bfloat16),
        ]
    )
    if size <= MANY:
        behind = [from_behind(packed, "sp", by) for by in range(1, size)]
    else:
        everything = lax.all_gather(packed, "sp")
        behind = [
            jnp.where(index >= by, jnp.take(everything, jnp.maximum(index - by, 0), axis=0), 0)
            for by in range(1, size)
        ]
    total = jnp.zeros((heads, width, entries), jnp.float32)
    for piece in reversed(behind):
        decay = piece[rows : rows + heads].astype(jnp.float32)
        state = piece[:rows].reshape(heads, width, entries).astype(jnp.float32)
        total = total * decay[:, None, :] + state
    return total.reshape(own_state.shape)


def from_behind(x, axis, by):
    size = lax.axis_size(axis)
    pairs = [(i, i + by) for i in range(size) if 0 <= i + by < size]
    return lax.ppermute(x, axis, pairs)


def causal_conv(signal, earlier, weights):
    kernel_len = weights.shape[0]
    length = signal.shape[0]
    joined = jnp.concatenate([earlier, signal], axis=0).astype(jnp.float32)
    accumulated = jnp.zeros((length, signal.shape[1]), jnp.float32)
    for offset in range(kernel_len):
        accumulated = accumulated + weights[offset][None, :] * joined[offset : offset + length]
    return jax.nn.silu(accumulated)


def device_states(scaled_in, log_attenuation, keys_b, queries_c, groups_here):
    length = scaled_in.shape[0]
    blocks = length // BLOCK
    per_group = scaled_in.shape[1] // groups_here
    scaled_in = scaled_in.reshape(blocks, BLOCK, groups_here, per_group, HEAD_DIM)
    log_attenuation = log_attenuation.reshape(blocks, BLOCK, groups_here, per_group)
    keys_b = keys_b.reshape(blocks, BLOCK, groups_here, STATE)
    queries_c = queries_c.reshape(blocks, BLOCK, groups_here, STATE)
    running = jnp.cumsum(log_attenuation, axis=1)
    lower_mask = jnp.tril(jnp.ones((BLOCK, BLOCK), dtype=bool))
    between = running[:, :, None] - running[:, None, :]
    decays = jnp.exp(jnp.where(lower_mask[None, :, :, None, None], between, -jnp.inf))
    scores = jnp.einsum("blgn,bsgn->blsg", queries_c, keys_b, precision=HIGHEST)
    inside = jnp.einsum("blsg,blsgr,bsgrp->blgrp", scores, decays, scaled_in, precision=HIGHEST)
    totals = running[:, -1]
    remain = jnp.exp(totals[:, None] - running)
    block_states = jnp.einsum(
        "bsgn,bsgr,bsgrp->bgrpn", keys_b, remain, scaled_in, precision=HIGHEST
    )

    def advance(carried, pieces):
        return (carried * jnp.exp(pieces[1])[..., None, None] + pieces[0], carried)

    initial = jnp.zeros(block_states.shape[1:], jnp.float32)
    own_state, entering = lax.scan(advance, initial, (block_states, totals))
    own_decay = jnp.exp(jnp.sum(totals, axis=0))
    incoming = incoming_states(own_state, own_decay)
    preceding = jnp.exp(jnp.cumsum(totals, axis=0) - totals)
    entering = entering + preceding[..., None, None] * incoming[None]
    outside = jnp.einsum(
        "blgn,bgrpn,blgr->blgrp", queries_c, entering, jnp.exp(running), precision=HIGHEST
    )
    return (inside + outside).reshape(length, -1)


def sp_exchange(pieces, sign):
    size, index = (lax.axis_size("sp"), lax.axis_index("sp"))
    if size <= MANY:
        return [pieces[0]] + [shifted(pieces[m], "sp", sign * m) for m in range(1, size)]
    places = jnp.arange(size, dtype=jnp.int32)
    sent = jnp.take(pieces, (sign * (places - index)) % size, axis=0)
    came = lax.all_to_all(sent, "sp", split_axis=0, concat_axis=0, tiled=True)
    came = jnp.take(came, (index - sign * places) % size, axis=0)
    return [came[m] for m in range(size)]


def to_experts(pieces):
    return sp_exchange(pieces, 1)


def from_experts(pieces):
    return sp_exchange(pieces, -1)


def near_order(size):
    order, bit = ([0], size // 2)
    while bit:
        order = order + [m | bit for m in order]
        bit //= 2
    return order


def gather_near(x, axis):
    bit = lax.axis_size("tp") // 2
    blocks, width = ([x], x.shape[axis])
    while bit:
        came = flipped(jnp.concatenate(blocks, axis=axis), "tp", bit)
        blocks = blocks + [
            lax.slice_in_dim(came, i * width, (i + 1) * width, axis=axis)
            for i in range(len(blocks))
        ]
        bit //= 2
    return blocks


def ordered(blocks, index):
    by = dict(zip(near_order(len(blocks)), blocks))
    bit = 1
    while bit < len(blocks):
        here = (index & bit) != 0
        by = {m: jnp.where(here, by[m ^ bit], by[m]) for m in by}
        bit *= 2
    return [by[m] for m in range(len(blocks))]


def per_device(
    carryover_vector,
    channel_source_entries,
    final_modulation_vector,
    entering_basis_matrix,
    readout_basis_matrix,
    raw_stride_amount,
    extra_log_attenuation,
    channel_fading_rate,
    channel_source_kernel,
    entering_basis_kernel,
    readout_basis_kernel,
    modulated_rescaling_vector,
    blender_final_matrix,
    specialist_rescaling_vector,
    specialist_gating_matrices,
    widening_matrices,
    contracting_matrices,
    assigned_specialist_ids,
    specialist_choice_affinity,
    cluster_chance,
):
    length, head_cols = channel_source_entries.shape
    row_count, model_width = carryover_vector.shape
    heads_here = channel_fading_rate.shape[0]
    state_cols = entering_basis_matrix.shape[1]
    groups_here = state_cols // STATE
    sp_count, sp_index = (lax.axis_size("sp"), lax.axis_index("sp"))
    tp_count, tp_index = (lax.axis_size("tp"), lax.axis_index("tp"))
    rim_rows = channel_source_kernel.shape[0] - 1
    local_experts = specialist_gating_matrices.shape[0]
    experts = sp_count * local_experts
    picks = assigned_specialist_ids.shape[1]
    capacity = 2 * row_count * picks // experts
    slots = min(local_experts * capacity, capacity * (experts // EGROUPS) // picks)

    everything = jnp.concatenate(
        [channel_source_entries, entering_basis_matrix, readout_basis_matrix], axis=1
    )
    neighbours = from_behind(everything[length - rim_rows :], "sp", 1)

    member = jnp.any(
        ((assigned_specialist_ids // local_experts - sp_index) % sp_count)[:, :, None]
        == jnp.arange(sp_count, dtype=jnp.int32),
        axis=1,
    )
    row = jnp.arange(length, dtype=jnp.int32)
    earlier = (row[:, None] > row[None, :]) & (
        row[:, None] // row_count == row[None, :] // row_count
    )
    rank = jnp.dot(
        earlier.astype(jnp.bfloat16),
        member.astype(jnp.bfloat16),
        preferred_element_type=jnp.float32,
    ).astype(jnp.int32)
    place = jnp.where(member, rank + (row // row_count * slots)[:, None], -1)
    own_place = lax.dynamic_slice_in_dim(
        jnp.where(member, rank, -1), tp_index * row_count, row_count, 0
    )
    pick_own = (
        own_place.T[:, None, :] == jnp.arange(slots, dtype=jnp.int32)[None, :, None]
    ).astype(jnp.bfloat16)
    pick_own = pick_own.reshape(sp_count * slots, row_count)
    pick_all = (
        place.T[:, None, :] == jnp.arange(tp_count * slots, dtype=jnp.int32)[None, :, None]
    ).astype(jnp.bfloat16)

    lifted = jnp.exp(specialist_choice_affinity)
    shares = cluster_chance[:, None] * lifted / jnp.sum(lifted, axis=1, keepdims=True)
    shares_high = shares.astype(jnp.bfloat16)
    shares_low = (shares - shares_high.astype(jnp.float32)).astype(jnp.bfloat16)
    own_ids = lax.dynamic_slice_in_dim(assigned_specialist_ids, tp_index * row_count, row_count, 0)
    notes = jnp.concatenate([shares_high, shares_low, own_ids.astype(jnp.bfloat16)], axis=1)
    notes = jnp.pad(notes, ((0, 0), (0, 128 - 3 * picks)))
    early = jnp.dot(
        pick_own,
        jnp.concatenate([carryover_vector, notes], axis=1),
        preferred_element_type=jnp.float32,
    ).astype(jnp.bfloat16)
    early = to_experts(early.reshape(sp_count, slots, model_width + 128))
    early = gather_near(jnp.concatenate(early, axis=0), 0)
    carried = jnp.concatenate(early, axis=0)

    weights = jnp.concatenate(
        [channel_source_kernel, entering_basis_kernel, readout_basis_kernel], axis=1
    )
    mixed_in = causal_conv(everything, neighbours, weights)
    inputs_x = mixed_in[:, :head_cols]
    keys_b = mixed_in[:, head_cols : head_cols + state_cols]
    queries_c = mixed_in[:, head_cols + state_cols :]
    channel_stride_amount = jax.nn.softplus(raw_stride_amount)
    log_attenuation = extra_log_attenuation - channel_fading_rate[None, :] * channel_stride_amount
    heads_x = inputs_x.reshape(length, heads_here, HEAD_DIM)
    mixed = device_states(
        heads_x * channel_stride_amount[:, :, None], log_attenuation, keys_b, queries_c, groups_here
    )
    gated = (mixed * jax.nn.silu(final_modulation_vector.astype(jnp.float32))).astype(jnp.bfloat16)

    routed = jnp.einsum("mrt,tc->mrc", pick_all, gated, preferred_element_type=jnp.float32)
    routed = to_experts(routed.astype(jnp.bfloat16))
    routed = jnp.stack(routed).reshape(sp_count, tp_count, slots, head_cols)
    routed = routed.transpose(1, 0, 2, 3).reshape(tp_count * sp_count * slots, head_cols)
    routed = ordered(gather_near(routed, 1), tp_index)
    routed = jnp.concatenate(routed, axis=1)
    near_rows = sp_count * slots
    routed = jnp.concatenate(
        [
            lax.dynamic_slice_in_dim(routed, (tp_index ^ m) * near_rows, near_rows, 0)
            for m in near_order(tp_count)
        ],
        axis=0,
    ).astype(jnp.float32)
    scale = lax.rsqrt(jnp.mean(routed * routed, axis=1, keepdims=True) + EPS)
    normed = (routed * scale * modulated_rescaling_vector[None, :]).astype(jnp.bfloat16)
    residual = carried[:, :model_width].astype(jnp.float32)
    middle = (
        residual + jnp.dot(normed, blender_final_matrix, preferred_element_type=jnp.float32)
    ).astype(jnp.bfloat16)
    middle_wide = middle.astype(jnp.float32)
    expert_input = (
        middle_wide
        * lax.rsqrt(jnp.mean(middle_wide * middle_wide, axis=1, keepdims=True) + EPS)
        * specialist_rescaling_vector[None, :]
    ).astype(jnp.bfloat16)

    notes = carried[:, model_width:].astype(jnp.float32)
    row_shares = notes[:, :picks] + notes[:, picks : 2 * picks]
    row_ids = notes[:, 2 * picks : 3 * picks].astype(jnp.int32) - sp_index * local_experts
    hidden = []
    for expert in range(local_experts):
        gate_value = jnp.dot(
            expert_input, specialist_gating_matrices[expert], preferred_element_type=jnp.float32
        )
        up_value = jnp.dot(
            expert_input, widening_matrices[expert], preferred_element_type=jnp.float32
        )
        share = jnp.sum(jnp.where(row_ids == expert, row_shares, 0.0), axis=1, keepdims=True)
        hidden.append((jax.nn.silu(gate_value) * up_value * share).astype(jnp.bfloat16))
    hidden = jnp.concatenate(hidden, axis=1)
    down = contracting_matrices.reshape(-1, model_width)
    order = near_order(tp_count)
    blocks = {
        m: jnp.dot(
            hidden[at * near_rows : (at + 1) * near_rows], down, preferred_element_type=jnp.float32
        )
        for at, m in enumerate(order)
    }
    bit = 1
    while bit < tp_count:
        away = sorted(m for m in blocks if m & bit)
        came = flipped(
            jnp.concatenate([blocks[m].astype(jnp.bfloat16) for m in away]), "tp", bit
        )
        blocks = {
            m ^ bit: blocks[m ^ bit]
            + came[at * near_rows : (at + 1) * near_rows].astype(jnp.float32)
            for at, m in enumerate(away)
        }
        bit *= 2
    first = (row_ids[:near_rows, :1] >= 0) & (row_ids[:near_rows, :1] < local_experts)
    answer = (blocks[0] + jnp.where(first, middle_wide[:near_rows], 0.0)).astype(jnp.bfloat16)
    returned = from_experts(answer.reshape(sp_count, slots, model_width))
    return lax.dot_general(
        pick_own,
        jnp.concatenate(returned, axis=0),
        (((0,), (0,)), ((), ())),
        preferred_element_type=jnp.float32,
    ).astype(jnp.bfloat16)


def solution(mesh):
    return jax.shard_map(
        per_device,
        mesh=mesh,
        in_specs=(
            P(("grp", "sp", "tp"), None),
            P(("grp", "sp"), "tp"),
            P(("grp", "sp"), "tp"),
            P(("grp", "sp"), "tp"),
            P(("grp", "sp"), "tp"),
            P(("grp", "sp"), "tp"),
            P(("grp", "sp"), "tp"),
            P("tp"),
            P(None, "tp"),
            P(None, "tp"),
            P(None, "tp"),
            P(),
            P(),
            P(),
            P("sp", None, "tp"),
            P("sp", None, "tp"),
            P("sp", "tp", None),
            P(("grp", "sp"), None),
            P(("grp", "sp", "tp"), None),
            P(("grp", "sp", "tp")),
        ),
        out_specs=P(("grp", "sp", "tp"), None),
        check_vma=False,
    )
```

time: 321 us -> 133 us (0.41)
  waiting for transfers between devices: 165 us -> 44.2 us
  blocking collectives: 57.9 us -> 0 us
  between operations: 14.2 us -> 0.48 us
  starting transfers between devices: 16.9 us -> 30.5 us
  local copies, waits for them, and re-layouts: 26.1 us -> 20.8 us
    unnamed x4 -> x0, waiting for transfers between devices: 84.5 us -> none
    ppermute x0 -> x15, waiting for transfers between devices: none -> 44.2 us  [the longest x6 24.8 us: flipped(): lax.ppermute(x, axis, [(i, i ^ bit) for i in range(lax.axis_size(axis))])]
    all_gather x1 -> x0, waiting for transfers between devices: 32.5 us -> none  [per_device(): arrived = lax.all_gather(received, 'tp', axis=2, tiled=True)]
    all_to_all x1 -> x0, blocking collectives: 30 us -> none  [per_device(): lax.all_to_all(outgoing, 'sp', split_axis=0, concat_axis=0, tiled=True)]
    all_to_all x1 -> x0, waiting for transfers between devices: 24.9 us -> none  [per_device(): lax.all_to_all(width_total, 'sp', split_axis=0, concat_axis=0, tiled=True)]
    reduce_scatter x1 -> x0, waiting for transfers between devices: 22.6 us -> none  [per_device(): lax.psum_scatter(jnp.dot(normed, weight_rows, preferred_element_type=jnp....]
    ppermute x0 -> x15, starting transfers between devices: none -> 16.6 us  [the longest x9 11.4 us: shifted(): return lax.ppermute(x, axis, [(i, (i + by) % size) for i in range(size)])]
    all_gather x1 -> x0, blocking collectives: 13.9 us -> none  [prefix(): lax.all_gather(part.astype(kind), axis)]
  transfers between devices with their start and end apart: 7 -> 19, of which waited for: 4 -> 8; matrix products, arithmetic and copies ran while one was open for 6% -> 18% of each run, Pallas kernels for 0% -> 0%
where the time goes in v1:
time: 133 us; the launch traced here: 132 us
  waiting for transfers between devices  44.2 us (33%)
  starting transfers between devices  30.5 us (23%)
  local copies, waits for them, and re-layouts  20.8 us (16%)
  other arithmetic  18 us (14%)
  matrix products  18 us (14%)
    ppermute x6, waiting for transfers between devices, flipped(): lax.ppermute(x, axis, [(i, i ^ bit) for i in range(lax.axis_size(axis))])  24.8 us
    ppermute x9, waiting for transfers between devices, shifted(): return lax.ppermute(x, axis, [(i, (i + by) % size) for i in range(size)])  19.4 us
    ppermute x4, starting transfers between devices, from_behind(): return lax.ppermute(x, axis, pairs)  13.9 us
    ppermute x9, starting transfers between devices, shifted(): return lax.ppermute(x, axis, [(i, (i + by) % size) for i in range(size)])  11.4 us
    unnamed x35, local copies, waits for them, and re-layouts  9.95 us
    ppermute x6, starting transfers between devices, flipped(): lax.ppermute(x, axis, [(i, i ^ bit) for i in range(lax.axis_size(axis))])  5.24 us
    dynamic_update_slice x4, other arithmetic, device_states(): own_state, entering = lax.scan(advance, initial, (block_states, totals))  2.67 us
  transfers between devices with their start and end apart: 19, of which 8 were waited for; matrix products, arithmetic and copies ran while one was open for 18% of the time, Pallas kernels for 0%

profile of v1, /device:TPU:0, one launch (start us, length us, event | category | flops | bytes accessed | tf_op | source)
XLA Modules:
  0.0 132.1 jit_solution(11796753256922869656)
XLA Ops:
  0.0 1.1 constant_dynamic-update-slice_fusion.16
  1.1 0.9 constant_dynamic-update-slice_fusion.15
  1.9 0.9 constant_dynamic-update-slice_fusion.14
  2.8 5.0 %collective-permute-start.5 = (bf16[3,512]{1,0:T(4,128)(2,1)S(1)}, bf16[3,512]{1,0:T(4,128)(2,1)S(1)}, u32[]{:S(2)}, u32[]{:S(2)}) collective-permute-start(bf16[3,512]{1,0:T(4,128)(2,1)S(1)} %slice.218), channel_id=1, source_target_pairs={{0,4},{4,8},{8,12},{1,5},{5,9},{9,13},{2,6},{6,10},{10,14},{3,7},{... | collective-permute-start | bytes 9224 | tf_op jit(solution)/shard_map/ppermute | solution.py:58
  8.4 0.7 exponential_reduce_fusion
  9.1 0.8 fusion.112
  9.8 0.7 and_select_fusion
  11.6 0.7 constant_dynamic-update-slice_fusion.13
  12.3 0.7 constant_dynamic-update-slice_fusion.12
  13.0 0.7 constant_dynamic-update-slice_fusion.11
  13.6 0.7 subtract_convert_fusion
  14.5 0.8 compare_select_fusion
  17.5 2.0 %convolution_convert_fusion = bf16[128,2176]{1,0:T(8,128)(2,1)} fusion(pred[128,64]{1,0:T(32,128)(4,1)S(1)} %bitcast_compare_fusion, bf16[64,6]{1,0:T(8,128)(2,1)S(1)} %copy.73, bf16[64,2048]{1,0:T(8,128)(2,1)} %param.22), kind=kOutput, calls=%fused_computation.8 | convolution fusion | flops 36765696 | bytes 828160 | tf_op jit(solution)/shard_map/dot_general | solution.py:230
  20.3 0.7 copy.60
  21.0 0.7 copy.61
  22.6 1.3 %convolution_bitcast_fusion = f32[4,1,4,64,128]{4,3,2,1,0:T(8,128)S(1)} fusion(f32[4,64,128,1]{2,1,3,0:T(8,128)S(1)} %bitcast.151, f32[4,64,4,64]{1,3,2,0:T(8,128)S(1)} %copy.58, f32[4,64,4]{1,2,0:T(4,128)} %copy.61, f32[4,64,4]{1,2,0:T(4,128)S(1)} %copy.57), kind=kOutput, calls=%fused_computation.18 | convolution fusion | flops 100794368 | bytes 925696 | tf_op jit(solution)/shard_map/bsgn,bsgr,bsgrp->bgrpn/dot_general | solution.py:87
  23.9 5.6 %while.13 = (s32[]{:T(128)}, f32[1,4,64,128]{3,2,1,0:T(8,128)S(1)}, f32[4,1,4,64,128]{4,3,2,1,0:T(8,128)}, f32[4,1,4]{2,1,0:T(1,128)}, f32[4,1,4,64,128]{4,3,2,1,0:T(8,128)S(1)}, /*index=5*/s32[]{:T(128)}, s32[]{:T(128)}) while((s32[]{:T(128)}, f32[1,4,64,128]{3,2,1,0:T(8,128)S(1)}, f32[4,1,4,64,128]{4,3,2,1,0:T(8,128)}, ...), condition=%wide.region_4.5_spmd.clone, body=%wide.region_3.4_spmd.clone.sunk | while | flops 131075 | bytes 655516 | solution.py:95
  24.6 0.7 bitcast_dynamic-update-slice_fusion.2
  25.4 0.7 fusion.149
  27.4 0.7 bitcast_dynamic-update-slice_fusion.2
  29.6 1.5 %pad_maximum_fusion.11 = bf16[272,128]{1,0:T(8,128)(2,1)} fusion(bf16[256,128]{1,0:T(8,128)(2,1)S(1)} %bitcast.154, bf16[272]{0:T(512)(128)(2,1)} %fusion.111), kind=kLoop, calls=%fused_computation.148 | loop fusion | flops 139264 | bytes 135712 | tf_op jit(solution)/shard_map/concatenate | solution.py:33
  31.0 4.1 %collective-permute-start.8 = (bf16[272,128]{1,0:T(8,128)(2,1)}, bf16[272,128]{1,0:T(8,128)(2,1)}, u32[]{:S(2)}, u32[]{:S(2)}) collective-permute-start(bf16[272,128]{1,0:T(8,128)(2,1)} %pad_maximum_fusion.11), channel_id=1, source_target_pairs={{0,4},{4,8},{8,12},{1,5},{5,9},{9,13},{2,6},{6,10},{10,14},{3,7},{... | collective-permute-start | bytes 208904 | tf_op jit(solution)/shard_map/ppermute | solution.py:58
  35.1 2.9 %collective-permute-start.7 = (bf16[272,128]{1,0:T(8,128)(2,1)}, bf16[272,128]{1,0:T(8,128)(2,1)}, u32[]{:S(2)}, u32[]{:S(2)}) collective-permute-start(bf16[272,128]{1,0:T(8,128)(2,1)} %pad_maximum_fusion.11), channel_id=1, source_target_pairs={{0,8},{4,12},{1,9},{5,13},{2,10},{6,14},{3,11},{7,15},{16,24},{20,... | collective-permute-start | bytes 208904 | tf_op jit(solution)/shard_map/ppermute | solution.py:58
  38.1 1.9 %collective-permute-start.6 = (bf16[272,128]{1,0:T(8,128)(2,1)}, bf16[272,128]{1,0:T(8,128)(2,1)}, u32[]{:S(2)}, u32[]{:S(2)}) collective-permute-start(bf16[272,128]{1,0:T(8,128)(2,1)} %pad_maximum_fusion.11), channel_id=1, source_target_pairs={{0,12},{1,13},{2,14},{3,15},{16,28},{17,29},{18,30},{19,31}} | collective-permute-start | bytes 208904 | tf_op jit(solution)/shard_map/ppermute | solution.py:58
  40.4 0.7 slice_convert_fusion.2
  41.1 0.7 slice_convert_fusion.3
  41.8 0.8 slice.235
  42.6 0.8 slice.233
  43.5 0.7 convert_multiply_fusion.3
  44.2 0.8 slice.231
  45.1 2.4 %fusion.6 = f32[4,64,1,4,64]{4,1,3,0,2:T(8,128)S(1)} fusion(f32[4,64,128,1]{2,1,3,0:T(8,128)S(1)} %bitcast.150, f32[4,1,4,64,128]{4,3,2,1,0:T(8,128)S(1)} %copy-done.3, f32[4,64,128]{2,1,0:T(8,128)S(1)} %convert_add_fusion, f32[4,4]{1,0:T(4,128)} %subtract_exponential_fusion.1, f32[4,64,4]{1,2,0:T(4,128)} %copy.60), kind=kOutput, calls=%fused_computation.21 | convolution fusion | flops 100990976 | bytes 1052736 | tf_op jit(solution)/shard_map/blgn,bgrpn,blgr->blgrp/dot_general | solution.py:100
  47.5 1.8 %fusion.7 = f32[4,64,1,4,64]{4,1,3,0,2:T(8,128)S(1)} fusion(f32[4,64,1,4,64]{4,1,3,0,2:T(8,128)S(1)} %fusion.6, f32[4,64,4,64]{1,3,2,0:T(8,128)S(1)} %copy.58, f32[4,64,4]{1,2,0:T(4,128)S(1)} %copy.57, f32[4,64,4]{1,2,0:T(4,128)S(1)} %copy.55, f32[4,64,64]{2,1,0:T(8,128)S(1)} %copy.53, pred[64,64]{1,0:T(8,128)(4,1)} %iota_compare_fusion.4), kind=kOutput, calls=%fused_computation.22 | convolution fusion | flops 50659328 | bytes 864256 | tf_op jit(solution)/shard_map/blsg,blsgr,bsgrp->blgrp/dot_general | solution.py:84
  50.0 1.2 convolution_convert_fusion.4
  51.2 2.4 %collective-permute-start.11 = (bf16[128,256]{1,0:T(8,128)(2,1)S(1)}, bf16[128,256]{1,0:T(8,128)(2,1)S(1)}, u32[]{:S(2)}, u32[]{:S(2)}) collective-permute-start(bf16[128,256]{1,0:T(8,128)(2,1)S(1)} %get-tuple-element.106), channel_id=1, source_target_pairs={{0,12},{4,0},{8,4},{12,8},{1,13},{5,1},{9,5},{13,9},{2,14},{6,2},{... | collective-permute-start | bytes 196616 | tf_op jit(solution)/shard_map/ppermute | solution.py:19
  53.6 1.9 %collective-permute-start.9 = (bf16[128,256]{1,0:T(8,128)(2,1)S(1)}, bf16[128,256]{1,0:T(8,128)(2,1)S(1)}, u32[]{:S(2)}, u32[]{:S(2)}) collective-permute-start(bf16[128,256]{1,0:T(8,128)(2,1)S(1)} %get-tuple-element.108), channel_id=1, source_target_pairs={{0,4},{4,8},{8,12},{12,0},{1,5},{5,9},{9,13},{13,1},{2,6},{6,10},{... | collective-permute-start | bytes 196616 | tf_op jit(solution)/shard_map/ppermute | solution.py:19
  55.4 0.7 constant_dynamic-update-slice_fusion.4
  56.1 1.9 %collective-permute-start.2 = (bf16[32,2176]{1,0:T(8,128)(2,1)S(1)}, bf16[32,2176]{1,0:T(8,128)(2,1)S(1)}, u32[]{:S(2)}, u32[]{:S(2)}) collective-permute-start(bf16[32,2176]{1,0:T(8,128)(2,1)S(1)} %get-tuple-element.95), channel_id=1, source_target_pairs={{0,12},{4,0},{8,4},{12,8},{1,13},{5,1},{9,5},{13,9},{2,14},{6,2},{... | collective-permute-start | bytes 417800 | tf_op jit(solution)/shard_map/ppermute | solution.py:19
  58.1 1.1 collective-permute-start.1
  59.2 1.5 %collective-permute-done.10 = bf16[128,256]{1,0:T(8,128)(2,1)S(1)} collective-permute-done((bf16[128,256]{1,0:T(8,128)(2,1)S(1)}, bf16[128,256]{1,0:T(8,128)(2,1)S(1)}, u32[]{:S(2)}, u32[]{:S(2)}) %collective-permute-start.10) | collective-permute-done | bytes 65568 | tf_op jit(solution)/shard_map/ppermute | solution.py:19
  60.8 1.6 %collective-permute-start.12 = (bf16[512,256]{1,0:T(8,128)(2,1)S(1)}, bf16[512,256]{1,0:T(8,128)(2,1)S(1)}, u32[]{:S(2)}, u32[]{:S(2)}) collective-permute-start(bf16[512,256]{1,0:T(8,128)(2,1)S(1)} %bitcast.145), channel_id=1, source_target_pairs={{0,2},{1,3},{2,0},{3,1},{4,6},{5,7},{6,4},{7,5},{8,10},{9,11},{10,... | collective-permute-start | bytes 786440 | tf_op jit(solution)/shard_map/ppermute | solution.py:23
  62.3 9.5 %collective-permute-done.1 = bf16[32,2176]{1,0:T(8,128)(2,1)S(1)} collective-permute-done((bf16[32,2176]{1,0:T(8,128)(2,1)S(1)}, bf16[32,2176]{1,0:T(8,128)(2,1)S(1)}, u32[]{:S(2)}, u32[]{:S(2)}) %collective-permute-start.1) | collective-permute-done | bytes 139296 | tf_op jit(solution)/shard_map/ppermute | solution.py:19
  71.9 1.6 %collective-permute-start.3 = (bf16[128,2176]{1,0:T(8,128)(2,1)S(1)}, bf16[128,2176]{1,0:T(8,128)(2,1)S(1)}, u32[]{:S(2)}, u32[]{:S(2)}) collective-permute-start(bf16[128,2176]{1,0:T(8,128)(2,1)S(1)} %pad_maximum_fusion.3), channel_id=1, source_target_pairs={{0,2},{1,3},{2,0},{3,1},{4,6},{5,7},{6,4},{7,5},{8,10},{9,11},{10,... | collective-permute-start | bytes 1671176 | tf_op jit(solution)/shard_map/ppermute | solution.py:23
  73.4 0.7 constant_dynamic-update-slice_fusion.3
  74.8 0.7 constant_dynamic-update-slice_fusion.1
  75.4 0.9 pad_maximum_fusion.4
  76.3 9.4 %collective-permute-done.3 = bf16[128,2176]{1,0:T(8,128)(2,1)S(1)} collective-permute-done((bf16[128,2176]{1,0:T(8,128)(2,1)S(1)}, bf16[128,2176]{1,0:T(8,128)(2,1)S(1)}, u32[]{:S(2)}, u32[]{:S(2)}) %collective-permute-start.3) | collective-permute-done | bytes 557088 | tf_op jit(solution)/shard_map/ppermute | solution.py:23
  85.7 0.9 constant_dynamic-update-slice_fusion
  86.6 1.4 %copy-done.4 = bf16[512,2176]{1,0:T(8,128)(2,1)} copy-done((bf16[512,2176]{1,0:T(8,128)(2,1)}, bf16[512,2176]{1,0:T(8,128)(2,1)S(1)}, u32[]{:S(2)}) %copy-start.4) | copy-done | bytes 2228248
  88.0 1.4 %broadcast_select_fusion.7 = (bf16[512,256]{1,0:T(8,128)(2,1)S(1)}, bf16[512,256]{1,0:T(8,128)(2,1)S(1)}, bf16[512,256]{1,0:T(8,128)(2,1)S(1)}, bf16[512,256]{1,0:T(8,128)(2,1)S(1)}) fusion(pred[]{:T(512)S(6)} %ne.102, bf16[512,256]{1,0:T(8,128)(2,1)} %copy-done.1, bf16[512,512]{1,0:T(8,128)(2,1)} %collective-permute-done.13, pred[]{:T(512)S(6)} %ne.103, ...), kind=kLoop, calls=%fused_computation.128 | loop fusion | flops 1048576 | bytes 2097154 | tf_op jit(solution)/shard_map/jit(_where)/select_n | solution.py:151
  89.9 1.0 collective-permute-done.4
  91.3 2.6 %multiply_reduce_fusion = (f32[512]{0:T(512)S(1)}, f32[512,2048]{1,0:T(8,128)S(1)}) fusion(bf16[1024,2048]{1,0:T(8,128)(2,1)S(1)} %copy-done.9, f32[1024]{0:T(1024)S(1)} %copy-done.12, f32[512]{0:T(512)S(1)} %add_rsqrt_fusion.1, bf16[128,1024]{1,0:T(8,128)(2,1)S(1)} %get-tuple-element.84, bf16[128,1024]{1,0:T(8,128)(2,1)S(1)} %get-tuple-element.85, ...), kind=kOutput, calls=%fused_computation.6 | convolution fusion | flops 2159541760 | bytes 11542528 | tf_op jit(solution)/shard_map/dot_general | solution.py:272
  94.4 1.2 copy-done.10
  95.5 0.8 fusion.25
  96.3 0.8 fusion.38
  97.9 0.8 fusion.22
  98.7 0.8 fusion.35
  101.2 2.3 %collective-permute-done.14 = bf16[256,2048]{1,0:T(8,128)(2,1)S(1)} collective-permute-done((bf16[256,2048]{1,0:T(8,128)(2,1)S(1)}, bf16[256,2048]{1,0:T(8,128)(2,1)S(1)}, u32[]{:S(2)}, u32[]{:S(2)}) %collective-permute-start.14) | collective-permute-done | bytes 1048608 | tf_op jit(solution)/shard_map/ppermute | solution.py:23
  104.0 1.6 %collective-permute-start.15 = (bf16[128,2048]{1,0:T(8,128)(2,1)S(1)}, bf16[128,2048]{1,0:T(8,128)(2,1)S(1)}, u32[]{:S(2)}, u32[]{:S(2)}) collective-permute-start(bf16[128,2048]{1,0:T(8,128)(2,1)S(1)} %add_convert_fusion.1), channel_id=1, source_target_pairs={{0,2},{1,3},{2,0},{3,1},{4,6},{5,7},{6,4},{7,5},{8,10},{9,11},{10,... | collective-permute-start | bytes 1572872 | tf_op jit(solution)/shard_map/ppermute | solution.py:23
  106.1 12.1 %collective-permute-done.15 = bf16[128,2048]{1,0:T(8,128)(2,1)S(1)} collective-permute-done((bf16[128,2048]{1,0:T(8,128)(2,1)S(1)}, bf16[128,2048]{1,0:T(8,128)(2,1)S(1)}, u32[]{:S(2)}, u32[]{:S(2)}) %collective-permute-start.15) | collective-permute-done | bytes 524320 | tf_op jit(solution)/shard_map/ppermute | solution.py:23
  118.7 1.2 collective-permute-start.17
  119.8 2.8 %collective-permute-start.16 = (bf16[32,2048]{1,0:T(8,128)(2,1)S(1)}, bf16[32,2048]{1,0:T(8,128)(2,1)S(1)}, u32[]{:S(2)}, u32[]{:S(2)}) collective-permute-start(bf16[32,2048]{1,0:T(8,128)(2,1)S(1)} %get-tuple-element.102), channel_id=1, source_target_pairs={{0,12},{4,0},{8,4},{12,8},{1,13},{5,1},{9,5},{13,9},{2,14},{6,2},{... | collective-permute-start | bytes 393224 | tf_op jit(solution)/shard_map/ppermute | solution.py:19
  122.7 4.2 %collective-permute-done.18 = bf16[32,2048]{1,0:T(8,128)(2,1)S(1)} collective-permute-done((bf16[32,2048]{1,0:T(8,128)(2,1)S(1)}, bf16[32,2048]{1,0:T(8,128)(2,1)S(1)}, u32[]{:S(2)}, u32[]{:S(2)}) %collective-permute-start.18) | collective-permute-done | bytes 131104 | tf_op jit(solution)/shard_map/ppermute | solution.py:19
  126.9 4.2 %collective-permute-done.17 = bf16[32,2048]{1,0:T(8,128)(2,1)S(1)} collective-permute-done((bf16[32,2048]{1,0:T(8,128)(2,1)S(1)}, bf16[32,2048]{1,0:T(8,128)(2,1)S(1)}, u32[]{:S(2)}, u32[]{:S(2)}) %collective-permute-start.17) | collective-permute-done | bytes 131104 | tf_op jit(solution)/shard_map/ppermute | solution.py:19
  131.1 1.0 convolution_convert_fusion.3
  (109 shorter events, 16.3 us)
Async XLA Ops:
  0.0 99.5 %copy-start = (bf16[2,256,2048]{2,1,0:T(8,128)(2,1)S(1)}, bf16[2,256,2048]{2,1,0:T(8,128)(2,1)}, u32[]{:S(2)}) copy-start(bf16[2,256,2048]{2,1,0:T(8,128)(2,1)} %param.38) | copy-start | bytes 6291460
  2.8 18.9 %collective-permute-start.5 = (bf16[3,512]{1,0:T(4,128)(2,1)S(1)}, bf16[3,512]{1,0:T(4,128)(2,1)S(1)}, u32[]{:S(2)}, u32[]{:S(2)}) collective-permute-start(bf16[3,512]{1,0:T(4,128)(2,1)S(1)} %slice.218), channel_id=1, source_target_pairs={{0,4},{4,8},{8,12},{1,5},{5,9},{9,13},{2,6},{6,10},{10,14},{3,7},{... | collective-permute-start | bytes 9224 | tf_op jit(solution)/shard_map/ppermute | solution.py:58
  16.9 0.6 copy-start.6
  29.6 15.5 %copy-start.3 = (f32[4,1,4,64,128]{4,3,2,1,0:T(8,128)S(1)}, f32[4,1,4,64,128]{4,3,2,1,0:T(8,128)}, u32[]{:S(2)}) copy-start(f32[4,1,4,64,128]{4,3,2,1,0:T(8,128)} %get-tuple-element.33) | copy-start | bytes 1572868
  31.0 9.4 %collective-permute-start.8 = (bf16[272,128]{1,0:T(8,128)(2,1)}, bf16[272,128]{1,0:T(8,128)(2,1)}, u32[]{:S(2)}, u32[]{:S(2)}) collective-permute-start(bf16[272,128]{1,0:T(8,128)(2,1)} %pad_maximum_fusion.11), channel_id=1, source_target_pairs={{0,4},{4,8},{8,12},{1,5},{5,9},{9,13},{2,6},{6,10},{10,14},{3,7},{... | collective-permute-start | bytes 208904 | tf_op jit(solution)/shard_map/ppermute | solution.py:58
  35.1 6.0 %collective-permute-start.7 = (bf16[272,128]{1,0:T(8,128)(2,1)}, bf16[272,128]{1,0:T(8,128)(2,1)}, u32[]{:S(2)}, u32[]{:S(2)}) collective-permute-start(bf16[272,128]{1,0:T(8,128)(2,1)} %pad_maximum_fusion.11), channel_id=1, source_target_pairs={{0,8},{4,12},{1,9},{5,13},{2,10},{6,14},{3,11},{7,15},{16,24},{20,... | collective-permute-start | bytes 208904 | tf_op jit(solution)/shard_map/ppermute | solution.py:58
  38.1 5.4 %collective-permute-start.6 = (bf16[272,128]{1,0:T(8,128)(2,1)}, bf16[272,128]{1,0:T(8,128)(2,1)}, u32[]{:S(2)}, u32[]{:S(2)}) collective-permute-start(bf16[272,128]{1,0:T(8,128)(2,1)} %pad_maximum_fusion.11), channel_id=1, source_target_pairs={{0,12},{1,13},{2,14},{3,15},{16,28},{17,29},{18,30},{19,31}} | collective-permute-start | bytes 208904 | tf_op jit(solution)/shard_map/ppermute | solution.py:58
  49.3 6.2 %copy-start.2 = (bf16[128,2176]{1,0:T(8,128)(2,1)S(1)}, bf16[128,2176]{1,0:T(8,128)(2,1)}, u32[]{:S(2)}) copy-start(bf16[128,2176]{1,0:T(8,128)(2,1)} %convolution_convert_fusion) | copy-start | bytes 1671172
  51.2 8.0 %collective-permute-start.11 = (bf16[128,256]{1,0:T(8,128)(2,1)S(1)}, bf16[128,256]{1,0:T(8,128)(2,1)S(1)}, u32[]{:S(2)}, u32[]{:S(2)}) collective-permute-start(bf16[128,256]{1,0:T(8,128)(2,1)S(1)} %get-tuple-element.106), channel_id=1, source_target_pairs={{0,12},{4,0},{8,4},{12,8},{1,13},{5,1},{9,5},{13,9},{2,14},{6,2},{... | collective-permute-start | bytes 196616 | tf_op jit(solution)/shard_map/ppermute | solution.py:19
  53.6 7.2 %collective-permute-start.10 = (bf16[128,256]{1,0:T(8,128)(2,1)S(1)}, bf16[128,256]{1,0:T(8,128)(2,1)S(1)}, u32[]{:S(2)}, u32[]{:S(2)}) collective-permute-start(bf16[128,256]{1,0:T(8,128)(2,1)S(1)} %get-tuple-element.107), channel_id=1, source_target_pairs={{0,8},{4,12},{8,0},{12,4},{1,9},{5,13},{9,1},{13,5},{2,10},{6,14},... | collective-permute-start | bytes 196616 | tf_op jit(solution)/shard_map/ppermute | solution.py:19
  53.6 7.2 %collective-permute-start.9 = (bf16[128,256]{1,0:T(8,128)(2,1)S(1)}, bf16[128,256]{1,0:T(8,128)(2,1)S(1)}, u32[]{:S(2)}, u32[]{:S(2)}) collective-permute-start(bf16[128,256]{1,0:T(8,128)(2,1)S(1)} %get-tuple-element.108), channel_id=1, source_target_pairs={{0,4},{4,8},{8,12},{12,0},{1,5},{5,9},{9,13},{13,1},{2,6},{6,10},{... | collective-permute-start | bytes 196616 | tf_op jit(solution)/shard_map/ppermute | solution.py:19
  56.1 6.2 %collective-permute-start.2 = (bf16[32,2176]{1,0:T(8,128)(2,1)S(1)}, bf16[32,2176]{1,0:T(8,128)(2,1)S(1)}, u32[]{:S(2)}, u32[]{:S(2)}) collective-permute-start(bf16[32,2176]{1,0:T(8,128)(2,1)S(1)} %get-tuple-element.95), channel_id=1, source_target_pairs={{0,12},{4,0},{8,4},{12,8},{1,13},{5,1},{9,5},{13,9},{2,14},{6,2},{... | collective-permute-start | bytes 417800 | tf_op jit(solution)/shard_map/ppermute | solution.py:19
  58.1 13.7 %collective-permute-start.1 = (bf16[32,2176]{1,0:T(8,128)(2,1)S(1)}, bf16[32,2176]{1,0:T(8,128)(2,1)S(1)}, u32[]{:S(2)}, u32[]{:S(2)}) collective-permute-start(bf16[32,2176]{1,0:T(8,128)(2,1)S(1)} %get-tuple-element.96), channel_id=1, source_target_pairs={{0,8},{4,12},{8,0},{12,4},{1,9},{5,13},{9,1},{13,5},{2,10},{6,14},... | collective-permute-start | bytes 417800 | tf_op jit(solution)/shard_map/ppermute | solution.py:19
  59.2 12.6 %collective-permute-start = (bf16[32,2176]{1,0:T(8,128)(2,1)S(1)}, bf16[32,2176]{1,0:T(8,128)(2,1)S(1)}, u32[]{:S(2)}, u32[]{:S(2)}) collective-permute-start(bf16[32,2176]{1,0:T(8,128)(2,1)S(1)} %get-tuple-element.97), channel_id=1, source_target_pairs={{0,4},{4,8},{8,12},{12,0},{1,5},{5,9},{9,13},{13,1},{2,6},{6,10},{... | collective-permute-start | bytes 417800 | tf_op jit(solution)/shard_map/ppermute | solution.py:19
  60.8 14.7 %collective-permute-start.12 = (bf16[512,256]{1,0:T(8,128)(2,1)S(1)}, bf16[512,256]{1,0:T(8,128)(2,1)S(1)}, u32[]{:S(2)}, u32[]{:S(2)}) collective-permute-start(bf16[512,256]{1,0:T(8,128)(2,1)S(1)} %bitcast.145), channel_id=1, source_target_pairs={{0,2},{1,3},{2,0},{3,1},{4,6},{5,7},{6,4},{7,5},{8,10},{9,11},{10,... | collective-permute-start | bytes 786440 | tf_op jit(solution)/shard_map/ppermute | solution.py:23
  71.9 13.8 %collective-permute-start.3 = (bf16[128,2176]{1,0:T(8,128)(2,1)S(1)}, bf16[128,2176]{1,0:T(8,128)(2,1)S(1)}, u32[]{:S(2)}, u32[]{:S(2)}) collective-permute-start(bf16[128,2176]{1,0:T(8,128)(2,1)S(1)} %pad_maximum_fusion.3), channel_id=1, source_target_pairs={{0,2},{1,3},{2,0},{3,1},{4,6},{5,7},{6,4},{7,5},{8,10},{9,11},{10,... | collective-permute-start | bytes 1671176 | tf_op jit(solution)/shard_map/ppermute | solution.py:23
  75.4 11.1 %copy-start.1 = (bf16[512,256]{1,0:T(8,128)(2,1)}, bf16[512,256]{1,0:T(8,128)(2,1)S(1)}, u32[]{:S(2)}) copy-start(bf16[512,256]{1,0:T(8,128)(2,1)S(1)} %collective-permute-done.12) | copy-start | bytes 786436
  76.3 11.6 %collective-permute-start.13 = (bf16[512,512]{1,0:T(8,128)(2,1)}, bf16[512,512]{1,0:T(8,128)(2,1)}, u32[]{:S(2)}, u32[]{:S(2)}) collective-permute-start(bf16[512,512]{1,0:T(8,128)(2,1)} %pad_maximum_fusion.4), channel_id=1, source_target_pairs={{0,1},{1,0},{2,3},{3,2},{4,5},{5,4},{6,7},{7,6},{8,9},{9,8},{10,11... | collective-permute-start | bytes 1572872 | tf_op jit(solution)/shard_map/ppermute | solution.py:23
  86.6 1.4 %copy-start.4 = (bf16[512,2176]{1,0:T(8,128)(2,1)}, bf16[512,2176]{1,0:T(8,128)(2,1)S(1)}, u32[]{:S(2)}) copy-start(bf16[512,2176]{1,0:T(8,128)(2,1)S(1)} %get-tuple-element.92) | copy-start | bytes 6684676
  87.9 3.0 %collective-permute-start.4 = (bf16[256,2176]{1,0:T(8,128)(2,1)}, bf16[256,2176]{1,0:T(8,128)(2,1)S(1)}, u32[]{:S(2)}, u32[]{:S(2)}) collective-permute-start(bf16[256,2176]{1,0:T(8,128)(2,1)} %get-tuple-element.91), channel_id=1, source_target_pairs={{0,1},{1,0},{2,3},{3,2},{4,5},{5,4},{6,7},{7,6},{8,9},{9,8},{10,11... | collective-permute-start | bytes 3342344 | tf_op jit(solution)/shard_map/ppermute | solution.py:23
  88.0 3.3 %copy-start.9 = (bf16[1024,2048]{1,0:T(8,128)(2,1)S(1)}, bf16[1024,2048]{1,0:T(8,128)(2,1)}, u32[]{:S(2)}) copy-start(bf16[1024,2048]{1,0:T(8,128)(2,1)} %param.34) | copy-start | bytes 12582916
  89.4 1.6 %copy-start.5 = (bf16[512,2176]{1,0:T(8,128)(2,1)S(1)}, bf16[512,2176]{1,0:T(8,128)(2,1)}, u32[]{:S(2)}) copy-start(bf16[512,2176]{1,0:T(8,128)(2,1)} %copy-done.4) | copy-start | bytes 6684676
  89.6 1.7 %copy-start.12 = (f32[1024]{0:T(1024)S(1)}, f32[1024]{0:T(1024)}, u32[]{:S(2)}) copy-start(f32[1024]{0:T(1024)} %param.33) | copy-start | bytes 12292
  91.3 2.7 %copy-start.8 = (f32[2048]{0:T(1024)S(1)}, f32[2048]{0:T(1024)}, u32[]{:S(2)}) copy-start(f32[2048]{0:T(1024)} %param.35) | copy-start | bytes 24580
  94.0 1.6 %copy-start.10 = (bf16[2,2048,256]{2,1,0:T(8,128)(2,1)S(1)}, bf16[2,2048,256]{2,1,0:T(8,128)(2,1)}, u32[]{:S(2)}) copy-start(bf16[2,2048,256]{2,1,0:T(8,128)(2,1)} %param.36) | copy-start | bytes 6291460
  96.3 1.6 %copy-start.11 = (bf16[2,2048,256]{2,1,0:T(8,128)(2,1)S(1)}, bf16[2,2048,256]{2,1,0:T(8,128)(2,1)}, u32[]{:S(2)}) copy-start(bf16[2,2048,256]{2,1,0:T(8,128)(2,1)} %param.37) | copy-start | bytes 6291460
  100.6 2.9 %collective-permute-start.14 = (bf16[256,2048]{1,0:T(8,128)(2,1)S(1)}, bf16[256,2048]{1,0:T(8,128)(2,1)S(1)}, u32[]{:S(2)}, u32[]{:S(2)}) collective-permute-start(bf16[256,2048]{1,0:T(8,128)(2,1)S(1)} %pad_maximum_fusion.2), channel_id=1, source_target_pairs={{0,1},{1,0},{2,3},{3,2},{4,5},{5,4},{6,7},{7,6},{8,9},{9,8},{10,11... | collective-permute-start | bytes 3145736 | tf_op jit(solution)/shard_map/ppermute | solution.py:23
  104.0 14.3 %collective-permute-start.15 = (bf16[128,2048]{1,0:T(8,128)(2,1)S(1)}, bf16[128,2048]{1,0:T(8,128)(2,1)S(1)}, u32[]{:S(2)}, u32[]{:S(2)}) collective-permute-start(bf16[128,2048]{1,0:T(8,128)(2,1)S(1)} %add_convert_fusion.1), channel_id=1, source_target_pairs={{0,2},{1,3},{2,0},{3,1},{4,6},{5,7},{6,4},{7,5},{8,10},{9,11},{10,... | collective-permute-start | bytes 1572872 | tf_op jit(solution)/shard_map/ppermute | solution.py:23
  106.1 25.0 %copy-start.7 = (pred[128,64]{1,0:T(32,128)(4,1)S(1)}, pred[128,64]{1,0:T(32,128)(4,1)}, u32[]{:S(2)}) copy-start(pred[128,64]{1,0:T(32,128)(4,1)} %copy-done.6) | copy-start | bytes 24580
  118.6 8.3 %collective-permute-start.18 = (bf16[32,2048]{1,0:T(8,128)(2,1)S(1)}, bf16[32,2048]{1,0:T(8,128)(2,1)S(1)}, u32[]{:S(2)}, u32[]{:S(2)}) collective-permute-start(bf16[32,2048]{1,0:T(8,128)(2,1)S(1)} %get-tuple-element.100), channel_id=1, source_target_pairs={{0,4},{4,8},{8,12},{12,0},{1,5},{5,9},{9,13},{13,1},{2,6},{6,10},{... | collective-permute-start | bytes 393224 | tf_op jit(solution)/shard_map/ppermute | solution.py:19
  118.7 12.4 %collective-permute-start.17 = (bf16[32,2048]{1,0:T(8,128)(2,1)S(1)}, bf16[32,2048]{1,0:T(8,128)(2,1)S(1)}, u32[]{:S(2)}, u32[]{:S(2)}) collective-permute-start(bf16[32,2048]{1,0:T(8,128)(2,1)S(1)} %get-tuple-element.101), channel_id=1, source_target_pairs={{0,8},{4,12},{8,0},{12,4},{1,9},{5,13},{9,1},{13,5},{2,10},{6,14},... | collective-permute-start | bytes 393224 | tf_op jit(solution)/shard_map/ppermute | solution.py:19
  119.8 11.2 %collective-permute-start.16 = (bf16[32,2048]{1,0:T(8,128)(2,1)S(1)}, bf16[32,2048]{1,0:T(8,128)(2,1)S(1)}, u32[]{:S(2)}, u32[]{:S(2)}) collective-permute-start(bf16[32,2048]{1,0:T(8,128)(2,1)S(1)} %get-tuple-element.102), channel_id=1, source_target_pairs={{0,12},{4,0},{8,4},{12,8},{1,13},{5,1},{9,5},{13,9},{2,14},{6,2},{... | collective-permute-start | bytes 393224 | tf_op jit(solution)/shard_map/ppermute | solution.py:19

commit v2 on v1

v2 whole, which is shorter than its diff:
```python
import functools

import jax
import jax.numpy as jnp
from jax import lax
from jax.experimental import pallas as pl
from jax.experimental.pallas import tpu as pltpu
from jax.sharding import PartitionSpec as P


HEAD_DIM = 64
STATE = 128
EGROUPS = 4
MANY = 8
TAIL = 16


EPS = 1e-06
HIGHEST = lax.Precision.HIGHEST


def shifted(x, axis, by):
    size = lax.axis_size(axis)
    return lax.ppermute(x, axis, [(i, (i + by) % size) for i in range(size)])


def flipped(x, axis, bit):
    return lax.ppermute(x, axis, [(i, i ^ bit) for i in range(lax.axis_size(axis))])


def from_behind(x, axis, by):
    size = lax.axis_size(axis)
    pairs = [(i, i + by) for i in range(size) if 0 <= i + by < size]
    return lax.ppermute(x, axis, pairs)


def from_all_behind(x):
    size, index = (lax.axis_size("sp"), lax.axis_index("sp"))
    if size <= MANY:
        return [from_behind(x, "sp", by) for by in range(1, size)]
    everything = lax.all_gather(x, "sp")
    return [
        jnp.where(index >= by, jnp.take(everything, jnp.maximum(index - by, 0), axis=0), 0)
        for by in range(1, size)
    ]


def exact_dot(a, b):
    return jnp.dot(a, b, precision=HIGHEST, preferred_element_type=jnp.float32)


def exact_dot_t(a, b):
    return lax.dot_general(
        a, b, (((1,), (1,)), ((), ())), precision=HIGHEST, preferred_element_type=jnp.float32
    )


def spread(heads, cols):
    head = lax.broadcasted_iota(jnp.int32, (heads, cols), 0)
    col = lax.broadcasted_iota(jnp.int32, (heads, cols), 1)
    first = head * HEAD_DIM
    return jnp.where((col >= first) & (col < first + HEAD_DIM), 1.0, 0.0)


def pick_kernel(blocks, slots, per_dest, dests):
    def body(start_ref, ids_ref, pick_ref):
        ids = ids_ref[...]
        picks, length = ids.shape
        rows = length // blocks
        dest = lax.broadcasted_iota(jnp.int32, (dests, length), 0) + start_ref[0]
        low = jnp.where(dest >= dests, dest - dests, dest) * per_dest
        member = jnp.zeros((dests, length), jnp.bool_)
        for k in range(picks):
            one = jnp.broadcast_to(ids[k : k + 1], (dests, length))
            member = member | ((one >= low) & (one < low + per_dest))
        before = lax.broadcasted_iota(jnp.int32, (length, length), 0)
        after = lax.broadcasted_iota(jnp.int32, (length, length), 1)
        base = jnp.zeros((1, length), jnp.int32)
        block_first = jnp.zeros((length, length), jnp.int32)
        for q in range(1, blocks):
            block_first = jnp.where(after >= q * rows, q * rows, block_first)
            base = jnp.where(
                lax.broadcasted_iota(jnp.int32, (1, length), 1) >= q * rows, q * slots, base
            )
        earlier = jnp.where((before < after) & (before >= block_first), 1.0, 0.0)
        rank = jnp.dot(
            jnp.where(member, 1.0, 0.0).astype(jnp.bfloat16),
            earlier.astype(jnp.bfloat16),
            preferred_element_type=jnp.float32,
        ).astype(jnp.int32)
        place = jnp.where(member, rank + base, -1)
        slot = lax.broadcasted_iota(jnp.int32, (blocks * slots, length), 0)
        for m in range(dests):
            hit = jnp.where(slot == place[m : m + 1], 1.0, 0.0)
            pick_ref[m * blocks * slots : (m + 1) * blocks * slots, :] = hit.astype(jnp.bfloat16)

    return body


def pick_rows(ids_t, start, blocks, slots, per_dest, dests):
    length = ids_t.shape[1]
    return pl.pallas_call(
        pick_kernel(blocks, slots, per_dest, dests),
        out_shape=jax.ShapeDtypeStruct((dests * blocks * slots, length), jnp.bfloat16),
        in_specs=[pl.BlockSpec(memory_space=pltpu.SMEM), pl.BlockSpec(memory_space=pltpu.VMEM)],
        name="pick_rows",
    )(start, ids_t)


def tail_body(x_ref, b_ref, c_ref, out_ref):
    width, entries = (x_ref.shape[1], b_ref.shape[1])
    out_ref[:, :width] = x_ref[...]
    out_ref[:, width : width + entries] = b_ref[...]
    out_ref[:, width + entries :] = c_ref[...]


def tails(x, keys, queries):
    length = x.shape[0]
    return pl.pallas_call(
        tail_body,
        grid=(1,),
        in_specs=[
            pl.BlockSpec((TAIL, v.shape[1]), lambda i: (length // TAIL - 1, 0))
            for v in (x, keys, queries)
        ],
        out_specs=pl.BlockSpec((TAIL, x.shape[1] + 2 * keys.shape[1]), lambda i: (0, 0)),
        out_shape=jax.ShapeDtypeStruct((TAIL, x.shape[1] + 2 * keys.shape[1]), x.dtype),
        name="tails",
    )(x, keys, queries)


def conv_of(value_ref, tail, taps_ref, scratch_ref):
    length, cols = value_ref.shape
    taps = taps_ref[...]
    kernel_len = taps.shape[0]
    scratch_ref[:TAIL, :cols] = tail
    scratch_ref[TAIL:, :cols] = value_ref[...].astype(jnp.float32)
    total = jnp.zeros((length, cols), jnp.float32)
    for offset in range(kernel_len):
        first = TAIL - kernel_len + 1 + offset
        total = total + taps[offset : offset + 1] * scratch_ref[first : first + length, :cols]
    return total * jax.nn.sigmoid(total)


def states_body(
    x_ref, b_ref, c_ref, tail_ref, raw_ref, extra_ref, rate_ref, xt_ref, bt_ref, ct_ref,
    packed_ref, scaled_ref, keys_ref, queries_ref, run_ref, run_t_ref, grown_ref, scratch_ref,
):
    length, cols = x_ref.shape
    entries = b_ref.shape[1]
    groups = entries // STATE
    heads = raw_ref.shape[0]
    tail = tail_ref[...].astype(jnp.float32)
    inputs_x = conv_of(x_ref, tail[:, :cols], xt_ref, scratch_ref)
    keys = conv_of(b_ref, tail[:, cols : cols + entries], bt_ref, scratch_ref)
    queries_ref[...] = conv_of(c_ref, tail[:, cols + entries :], ct_ref, scratch_ref)
    keys_ref[...] = keys
    raw = raw_ref[...]
    stride = jnp.maximum(raw, 0.0) + jnp.log1p(jnp.exp(-jnp.abs(raw)))
    logs = extra_ref[...] - rate_ref[...] * stride
    row = lax.broadcasted_iota(jnp.int32, (length, length), 0)
    col = lax.broadcasted_iota(jnp.int32, (length, length), 1)
    running = exact_dot_t(jnp.where(row >= col, 1.0, 0.0), logs)
    run_ref[...] = running
    run_t_ref[...] = exact_dot(logs, jnp.where(row <= col, 1.0, 0.0))
    stride = exact_dot_t(jnp.where(row == col, 1.0, 0.0), stride)
    wide = spread(heads, cols)
    scaled = inputs_x * exact_dot(stride, wide)
    scaled_ref[...] = scaled
    grown_ref[...] = exact_dot(jnp.exp(running), wide)
    last = running[length - 1 :]
    remain = exact_dot(jnp.exp(last - running), wide)
    left = scaled * remain
    width = cols // groups
    for g in range(groups):
        packed_ref[:STATE, g * width : (g + 1) * width] = exact_dot(
            keys[:, g * STATE : (g + 1) * STATE].T, left[:, g * width : (g + 1) * width]
        ).astype(jnp.bfloat16)
    decay = exact_dot(jnp.broadcast_to(jnp.exp(last), (TAIL, heads)), wide)
    packed_ref[STATE:, :] = decay.astype(jnp.bfloat16)


def inside_body(scaled_ref, keys_ref, queries_ref, run_ref, run_t_ref, out_ref):
    length, cols = scaled_ref.shape
    heads = run_ref.shape[1]
    groups = keys_ref.shape[1] // STATE
    per_group = heads // groups
    scaled = scaled_ref[...]
    running = run_ref[...]
    running_t = run_t_ref[...]
    row = lax.broadcasted_iota(jnp.int32, (length, length), 0)
    col = lax.broadcasted_iota(jnp.int32, (length, length), 1)
    lower = row >= col
    wide = spread(heads, cols)
    total = jnp.zeros((length, cols), jnp.float32)
    for g in range(groups):
        scores = lax.dot_general(
            queries_ref[:, g * STATE : (g + 1) * STATE],
            keys_ref[:, g * STATE : (g + 1) * STATE],
            (((1,), (1,)), ((), ())),
            precision=HIGHEST,
            preferred_element_type=jnp.float32,
        )
        for h in range(g * per_group, (g + 1) * per_group):
            between = running[:, h : h + 1] - running_t[h : h + 1]
            decays = jnp.exp(jnp.where(lower, between, -jnp.inf))
            total = total + exact_dot(scores * decays, scaled * wide[h : h + 1])
    out_ref[...] = total


def gate_body(pieces, inside_ref, queries_ref, grown_ref, gate_ref, pick_ref, *rest):
    behind, out_refs, gated_ref = (rest[:pieces], rest[pieces:-1], rest[-1])
    _, cols = inside_ref.shape
    groups = queries_ref.shape[1] // STATE
    width = cols // groups
    total = jnp.zeros((STATE, cols), jnp.float32)
    for piece in reversed(behind):
        decay = piece[STATE:, :].astype(jnp.float32)[:1]
        total = total * decay + piece[:STATE, :].astype(jnp.float32)
    gate = gate_ref[...].astype(jnp.float32)
    gate = gate * jax.nn.sigmoid(gate)
    for g in range(groups):
        part = slice(g * width, (g + 1) * width)
        outside = exact_dot(queries_ref[:, g * STATE : (g + 1) * STATE], total[:, part])
        gated_ref[:, part] = (
            (inside_ref[:, part] + outside * grown_ref[:, part]) * gate[:, part]
        ).astype(jnp.bfloat16)
    gated = gated_ref[...]
    size = out_refs[0].shape[0]
    for m, out_ref in enumerate(out_refs):
        out_ref[...] = jnp.dot(
            pick_ref[m * size : (m + 1) * size, :], gated, preferred_element_type=jnp.float32
        ).astype(jnp.bfloat16)


def sp_exchange(pieces, sign):
    size, index = (lax.axis_size("sp"), lax.axis_index("sp"))
    if size <= MANY:
        return [pieces[0]] + [shifted(pieces[m], "sp", sign * m) for m in range(1, size)]
    places = jnp.arange(size, dtype=jnp.int32)
    sent = jnp.take(jnp.stack(list(pieces)), (sign * (places - index)) % size, axis=0)
    came = lax.all_to_all(sent, "sp", split_axis=0, concat_axis=0, tiled=True)
    came = jnp.take(came, (index - sign * places) % size, axis=0)
    return [came[m] for m in range(size)]


def to_experts(pieces):
    return sp_exchange(pieces, 1)


def near_order(size):
    order, bit = ([0], size // 2)
    while bit:
        order = order + [m | bit for m in order]
        bit //= 2
    return order


def gather_near(blocks, axis):
    bit, width = (lax.axis_size("tp") // 2 // len(blocks), blocks[0].shape[axis])
    while bit:
        came = flipped(jnp.concatenate(blocks, axis=axis), "tp", bit)
        blocks = blocks + [
            lax.slice_in_dim(came, i * width, (i + 1) * width, axis=axis)
            for i in range(len(blocks))
        ]
        bit //= 2
    return blocks


def ordered(blocks, index):
    by = dict(zip(near_order(len(blocks)), blocks))
    bit = 1
    while bit < len(blocks):
        here = (index & bit) != 0
        by = {m: jnp.where(here, by[m ^ bit], by[m]) for m in by}
        bit *= 2
    return [by[m] for m in range(len(blocks))]


def layer(
    carryover_vector,
    channel_source_entries,
    final_modulation_vector,
    entering_basis_matrix,
    readout_basis_matrix,
    raw_stride_amount,
    extra_log_attenuation,
    channel_fading_rate,
    channel_source_kernel,
    entering_basis_kernel,
    readout_basis_kernel,
    modulated_rescaling_vector,
    blender_final_matrix,
    specialist_rescaling_vector,
    specialist_gating_matrices,
    widening_matrices,
    contracting_matrices,
    assigned_specialist_ids,
    specialist_choice_affinity,
    cluster_chance,
):
    length, head_cols = channel_source_entries.shape
    row_count, model_width = carryover_vector.shape
    heads_here = channel_fading_rate.shape[0]
    state_cols = entering_basis_matrix.shape[1]
    sp_count, sp_index = (lax.axis_size("sp"), lax.axis_index("sp"))
    tp_count, tp_index = (lax.axis_size("tp"), lax.axis_index("tp"))
    local_experts = specialist_gating_matrices.shape[0]
    experts = sp_count * local_experts
    picks = assigned_specialist_ids.shape[1]
    capacity = 2 * row_count * picks // experts
    slots = min(local_experts * capacity, capacity * (experts // EGROUPS) // picks)

    tail = tails(channel_source_entries, entering_basis_matrix, readout_basis_matrix)
    tail, routing_ids = lax.optimization_barrier((tail, assigned_specialist_ids))
    neighbours = from_behind(tail, "sp", 1)

    start = sp_index.astype(jnp.int32).reshape(1)
    own_ids = lax.dynamic_slice_in_dim(routing_ids, tp_index * row_count, row_count, 0)
    pick_own = pick_rows(own_ids.T, start, 1, slots, local_experts, sp_count)
    pick_all = pick_rows(
        routing_ids.T, start, tp_count, slots, local_experts, sp_count
    )

    lifted = jnp.exp(specialist_choice_affinity)
    shares = cluster_chance[:, None] * lifted / jnp.sum(lifted, axis=1, keepdims=True)
    shares_high = shares.astype(jnp.bfloat16)
    shares_low = (shares - shares_high.astype(jnp.float32)).astype(jnp.bfloat16)
    notes = jnp.concatenate([shares_high, shares_low, own_ids.astype(jnp.bfloat16)], axis=1)
    notes = jnp.pad(notes, ((0, 0), (0, 128 - 3 * picks)))
    early = jnp.dot(
        pick_own,
        jnp.concatenate([carryover_vector, notes], axis=1),
        preferred_element_type=jnp.float32,
    ).astype(jnp.bfloat16)
    early = to_experts(early.reshape(sp_count, slots, model_width + 128))

    segment = jax.ShapeDtypeStruct((length, head_cols), jnp.float32)
    state_map = jax.ShapeDtypeStruct((length, state_cols), jnp.float32)
    packed, scaled, keys_b, queries_c, running, running_t, grown = pl.pallas_call(
        states_body,
        out_shape=(
            jax.ShapeDtypeStruct((STATE + TAIL, head_cols), jnp.bfloat16),
            segment,
            state_map,
            state_map,
            jax.ShapeDtypeStruct((length, heads_here), jnp.float32),
            jax.ShapeDtypeStruct((heads_here, length), jnp.float32),
            segment,
        ),
        scratch_shapes=[pltpu.VMEM((length + TAIL, max(head_cols, state_cols)), jnp.float32)],
        name="states",
    )(
        channel_source_entries,
        entering_basis_matrix,
        readout_basis_matrix,
        neighbours,
        raw_stride_amount.T,
        extra_log_attenuation.T,
        channel_fading_rate[:, None],
        channel_source_kernel,
        entering_basis_kernel,
        readout_basis_kernel,
    )
    packed, *early = lax.optimization_barrier((packed, *early))
    halves = (
        list(range(1, sp_count // 2 + 1)),
        list(range(sp_count // 2 + 1, sp_count)) + [0],
    )
    early = jnp.concatenate([early[m] for half in halves for m in half], axis=0)
    near_x = flipped(early, "tp", tp_count // 2)
    behind = from_all_behind(packed)
    inside = pl.pallas_call(inside_body, out_shape=segment, name="inside")(
        scaled, keys_b, queries_c, running, running_t
    )
    routed = pl.pallas_call(
        functools.partial(gate_body, len(behind)),
        out_shape=[
            jax.ShapeDtypeStruct((tp_count * slots, head_cols), jnp.bfloat16)
            for _ in range(sp_count)
        ],
        scratch_shapes=[pltpu.VMEM((length, head_cols), jnp.bfloat16)],
        name="gate",
    )(inside, queries_c, grown, final_modulation_vector, pick_all, *behind)

    routed = to_experts(routed)
    *routed, near_x = lax.optimization_barrier((*routed, near_x))
    carried = gather_near([early, near_x], 0)
    ends = [0]
    for half in halves:
        ends.append(ends[-1] + len(half) * slots)
    carried = jnp.concatenate(
        [block[lo:hi] for lo, hi in zip(ends, ends[1:]) for block in carried], axis=0
    )
    routed = jnp.concatenate(
        [
            jnp.stack([routed[m].reshape(tp_count, slots, head_cols) for m in half], axis=1)
            .reshape(tp_count * len(half) * slots, head_cols)
            for half in halves
        ]
    )
    routed = ordered(gather_near([routed], 1), tp_index)
    routed = jnp.concatenate(routed, axis=1)
    order = near_order(tp_count)
    sizes = [len(half) * slots for half in halves]
    routed = jnp.concatenate(
        [
            lax.dynamic_slice_in_dim(routed, tp_count * lo + (tp_index ^ m) * size, size, 0)
            for lo, size in zip(ends, sizes)
            for m in order
        ],
        axis=0,
    ).astype(jnp.float32)
    scale = lax.rsqrt(jnp.mean(routed * routed, axis=1, keepdims=True) + EPS)
    normed = (routed * scale * modulated_rescaling_vector[None, :]).astype(jnp.bfloat16)
    residual = carried[:, :model_width].astype(jnp.float32)
    middle = (
        residual + jnp.dot(normed, blender_final_matrix, preferred_element_type=jnp.float32)
    ).astype(jnp.bfloat16)
    middle_wide = middle.astype(jnp.float32)
    expert_input = (
        middle_wide
        * lax.rsqrt(jnp.mean(middle_wide * middle_wide, axis=1, keepdims=True) + EPS)
        * specialist_rescaling_vector[None, :]
    ).astype(jnp.bfloat16)

    notes = carried[:, model_width:].astype(jnp.float32)
    row_shares = notes[:, :picks] + notes[:, picks : 2 * picks]
    row_ids = notes[:, 2 * picks : 3 * picks].astype(jnp.int32) - sp_index * local_experts
    hidden = []
    for expert in range(local_experts):
        gate_value = jnp.dot(
            expert_input, specialist_gating_matrices[expert], preferred_element_type=jnp.float32
        )
        up_value = jnp.dot(
            expert_input, widening_matrices[expert], preferred_element_type=jnp.float32
        )
        share = jnp.sum(jnp.where(row_ids == expert, row_shares, 0.0), axis=1, keepdims=True)
        hidden.append((jax.nn.silu(gate_value) * up_value * share).astype(jnp.bfloat16))
    hidden = jnp.concatenate(hidden, axis=1)
    down = contracting_matrices.reshape(-1, model_width)
    returned = [None] * sp_count
    for lo, size, half in zip(ends, sizes, halves):
        base = tp_count * lo
        blocks = {
            m: jnp.dot(
                hidden[base + at * size : base + (at + 1) * size],
                down,
                preferred_element_type=jnp.float32,
            )
            for at, m in enumerate(order)
        }
        bit = 1
        while bit < tp_count:
            away = sorted(m for m in blocks if m & bit)
            came = flipped(
                jnp.concatenate([blocks[m].astype(jnp.bfloat16) for m in away]), "tp", bit
            )
            blocks = {
                m ^ bit: blocks[m ^ bit] + came[at * size : (at + 1) * size].astype(jnp.float32)
                for at, m in enumerate(away)
            }
            bit *= 2
        first = row_ids[base : base + size, :1]
        first = (first >= 0) & (first < local_experts)
        answer = blocks[0] + jnp.where(first, middle_wide[base : base + size], 0.0)
        answer = answer.astype(jnp.bfloat16).reshape(len(half), slots, model_width)
        for at, m in enumerate(half):
            if sp_count <= MANY and m:
                returned[m] = shifted(answer[at], "sp", -m)
            else:
                returned[m] = answer[at]
    if sp_count > MANY:
        returned = sp_exchange(returned, -1)
    return lax.dot_general(
        pick_own,
        jnp.concatenate(returned, axis=0),
        (((0,), (0,)), ((), ())),
        preferred_element_type=jnp.float32,
    ).astype(jnp.bfloat16)


def solution(mesh):
    return jax.shard_map(
        layer,
        mesh=mesh,
        in_specs=(
            P(("grp", "sp", "tp"), None),
            P(("grp", "sp"), "tp"),
            P(("grp", "sp"), "tp"),
            P(("grp", "sp"), "tp"),
            P(("grp", "sp"), "tp"),
            P(("grp", "sp"), "tp"),
            P(("grp", "sp"), "tp"),
            P("tp"),
            P(None, "tp"),
            P(None, "tp"),
            P(None, "tp"),
            P(),
            P(),
            P(),
            P("sp", None, "tp"),
            P("sp", None, "tp"),
            P("sp", "tp", None),
            P(("grp", "sp"), None),
            P(("grp", "sp", "tp"), None),
            P(("grp", "sp", "tp")),
        ),
        out_specs=P(("grp", "sp", "tp"), None),
        check_vma=False,
    )
```

time: 133 us -> 110 us (0.83)
  Pallas kernels: 0 us -> 14.4 us
  other arithmetic: 18 us -> 6.69 us
  local copies, waits for them, and re-layouts: 20.8 us -> 9.54 us
  waiting for transfers between devices: 44.2 us -> 33.5 us
  matrix products: 18 us -> 12.2 us
  starting transfers between devices: 30.5 us -> 33 us
    pallas_call x0 -> x6, Pallas kernels: none -> 14.4 us  [the longest x1 3.8 us: layer(): pl.pallas_call(states_body, out_shape=(jax.ShapeDtypeStruct((STATE + TAIL...]
    ppermute x6 -> x8, waiting for transfers between devices: 24.8 us -> 17.7 us  [flipped(): lax.ppermute(x, axis, [(i, i ^ bit) for i in range(lax.axis_size(axis))])]
    dot_general x17 -> x15, matrix products: 18 us -> 12.2 us  [the longest x8 4.32 us: layer(): jnp.dot(hidden[base + at * size:base + (at + 1) * size], down, preferred_...]
    ppermute x9, waiting for transfers between devices: 19.4 us -> 14.1 us  [shifted(): return lax.ppermute(x, axis, [(i, (i + by) % size) for i in range(size)])]
    exp x6 -> x0, local copies, waits for them, and re-layouts: 3.94 us -> none  [the longest x4 2.55 us: advance(): return (carried * jnp.exp(pieces[1])[..., None, None] + pieces[0], carried)]
    dynamic_update_slice x4 -> x0, other arithmetic: 2.67 us -> none  [device_states(): own_state, entering = lax.scan(advance, initial, (block_states, totals))]
    slice x9 -> x3, local copies, waits for them, and re-layouts: 2.64 us -> 0.08 us  [the longest x1 0.05 us: sp_exchange(): pieces[m]]
    ppermute x9, starting transfers between devices: 11.4 us -> 13.6 us  [shifted(): return lax.ppermute(x, axis, [(i, (i + by) % size) for i in range(size)])]
  transfers between devices with their start and end apart: 19 -> 21, of which waited for: 8 -> 10; matrix products, arithmetic and copies ran while one was open for 18% -> 7% of each run, Pallas kernels for 0% -> 11%
where the time goes in v2:
time: 110 us
  waiting for transfers between devices  33.5 us (30%)
  starting transfers between devices  33 us (30%)
  Pallas kernels  14.4 us (13%)
  matrix products  12.2 us (11%)
  local copies, waits for them, and re-layouts  9.54 us (9%)
  other arithmetic  6.69 us (6%)
    ppermute x8, waiting for transfers between devices, flipped(): lax.ppermute(x, axis, [(i, i ^ bit) for i in range(lax.axis_size(axis))])  17.7 us
    ppermute x9, waiting for transfers between devices, shifted(): return lax.ppermute(x, axis, [(i, (i + by) % size) for i in range(size)])  14.1 us
    ppermute x4, starting transfers between devices, from_behind(): return lax.ppermute(x, axis, pairs)  13.8 us
    ppermute x9, starting transfers between devices, shifted(): return lax.ppermute(x, axis, [(i, (i + by) % size) for i in range(size)])  13.6 us
    unnamed x49, local copies, waits for them, and re-layouts  7.91 us
    ppermute x8, starting transfers between devices, flipped(): lax.ppermute(x, axis, [(i, i ^ bit) for i in range(lax.axis_size(axis))])  5.54 us
    dot_general x8, matrix products, layer(): jnp.dot(hidden[base + at * size:base + (at + 1) * size], down, preferred_...  4.32 us
    pallas_call x1, Pallas kernels, layer(): pl.pallas_call(states_body, out_shape=(jax.ShapeDtypeStruct((STATE + TAIL...  3.8 us
  transfers between devices with their start and end apart: 21, of which 10 were waited for; matrix products, arithmetic and copies ran while one was open for 7% of the time, Pallas kernels for 11%

profile of v2, /device:TPU:0, one launch (start us, length us, event | category | flops | bytes accessed | tf_op | source)
XLA Modules:
  0.0 109.9 jit_solution(9784509313730161711)
XLA Ops:
  0.0 0.9 exponential_reduce_fusion
  0.9 1.3 %tails.1 = bf16[16,512]{1,0:T(8,128)(2,1)} custom-call(bf16[256,256]{1,0:T(8,128)(2,1)} %x_ref.3, bf16[256,128]{1,0:T(8,128)(2,1)} %b_ref.3, bf16[256,128]{1,0:T(8,128)(2,1)} %c_ref.3), custom_call_target="tpu_custom_call" | custom-call | tf_op jit(solution)/shard_map/tails/pallas_call | solution.py:119
  2.2 0.7 subtract_convert_fusion
  2.9 1.3 %fusion.64 = (bf16[64,2]{0,1:T(2,128)(2,1)S(1)}, s32[2,64]{1,0:T(2,128)}) fusion(s32[256,2]{0,1:T(2,128)} %param.37, s32[]{:T(128)S(6)} %select_n.79), kind=kLoop, calls=%fused_computation.137 | loop fusion | flops 128 | bytes 1284 | tf_op jit(solution)/shard_map/convert_element_type | solution.py:330
  4.4 1.4 %pick_rows.2 = bf16[128,64]{1,0:T(8,128)(2,1)} custom-call(s32[1]{0:T(128)} %bitcast.start_ref, s32[2,64]{1,0:T(2,128)} %get-tuple-element.77.ids_ref), custom_call_target="tpu_custom_call" | custom-call | tf_op jit(solution)/shard_map/pick_rows/pallas_call | solution.py:102
  5.8 1.3 %convolution_convert_fusion = bf16[128,2176]{1,0:T(8,128)(2,1)S(1)} fusion(bf16[128,64]{1,0:T(8,128)(2,1)} %pick_rows.2, bf16[64,6]{1,0:T(8,128)(2,1)S(1)} %copy.29, bf16[64,2048]{1,0:T(8,128)(2,1)} %param.20), kind=kOutput, calls=%fused_computation.3 | convolution fusion | flops 36765696 | bytes 836352 | tf_op jit(solution)/shard_map/dot_general | solution.py:332
  7.1 5.1 %collective-permute-start.3 = (bf16[32,2176]{1,0:T(8,128)(2,1)S(1)}, bf16[32,2176]{1,0:T(8,128)(2,1)S(1)}, u32[]{:S(2)}, u32[]{:S(2)}) collective-permute-start(bf16[32,2176]{1,0:T(8,128)(2,1)S(1)} %get-tuple-element.64), channel_id=1, source_target_pairs={{0,12},{4,0},{8,4},{12,8},{1,13},{5,1},{9,5},{13,9},{2,14},{6,2},{... | collective-permute-start | bytes 417800 | tf_op jit(solution)/shard_map/ppermute | solution.py:24
  12.2 1.0 collective-permute-start.1
  13.3 4.4 %collective-permute-start = (bf16[16,512]{1,0:T(8,128)(2,1)S(1)}, bf16[16,512]{1,0:T(8,128)(2,1)S(1)}, u32[]{:S(2)}, u32[]{:S(2)}) collective-permute-start(bf16[16,512]{1,0:T(8,128)(2,1)S(1)} %copy-done.7), channel_id=1, source_target_pairs={{0,4},{4,8},{8,12},{1,5},{5,9},{9,13},{2,6},{6,10},{10,14},{3,7},{... | collective-permute-start | bytes 49160 | tf_op jit(solution)/shard_map/ppermute | solution.py:34
  17.7 0.7 copy.23.rate_ref
  18.3 1.6 %pick_rows.3.pick_ref = bf16[512,256]{1,0:T(8,128)(2,1)} custom-call(s32[1]{0:T(128)} %bitcast.start_ref, s32[2,256]{1,0:T(2,128)} %bitcast.67), custom_call_target="tpu_custom_call" | custom-call | tf_op jit(solution)/shard_map/pick_rows/pallas_call | solution.py:102
  19.9 1.6 %collective-permute-done.tail_ref = bf16[16,512]{1,0:T(8,128)(2,1)S(1)} collective-permute-done((bf16[16,512]{1,0:T(8,128)(2,1)S(1)}, bf16[16,512]{1,0:T(8,128)(2,1)S(1)}, u32[]{:S(2)}, u32[]{:S(2)}) %collective-permute-start) | collective-permute-done | bytes 16416 | tf_op jit(solution)/shard_map/ppermute | solution.py:34
  21.6 0.6 copy-done.8
  22.2 3.8 %states.1 = (bf16[144,256]{1,0:T(8,128)(2,1)}, f32[256,256]{1,0:T(8,128)}, f32[256,128]{1,0:T(8,128)}, f32[256,128]{1,0:T(8,128)}, f32[256,4]{1,0:T(8,128)}, /*index=5*/f32[4,256]{1,0:T(4,128)}, f32[256,256]{1,0:T(8,128)}) custom-call(bf16[256,256]{1,0:T(8,128)(2,1)} %x_ref.3, bf16[256,128]{1,0:T(8,128)(2,1)} %b_ref.3, bf16[256,128]{1,0:T(8,128)(2,1)} %c_ref.3, ...), custom_call_target="tpu_custom_call" | custom-call | tf_op jit(solution)/shard_map/states/pallas_call | solution.py:341
  26.0 3.6 %inside.1.inside_ref = f32[256,256]{1,0:T(8,128)} custom-call(f32[256,256]{1,0:T(8,128)} %get-tuple-element.33.scaled_ref, f32[256,128]{1,0:T(8,128)} %get-tuple-element.34.keys_ref, f32[256,128]{1,0:T(8,128)} %get-tuple-element.35.queries_ref, f32[256,4]{1,0:T(8,128)} %get-tuple-element.36.run_ref, f32[4,256]{1,0:T(4,128)} %get-tuple-element.37.run_t_ref), custom_call_target="tpu_custom_call" | custom-call | tf_op jit(solution)/shard_map/inside/pallas_call | solution.py:374
  29.5 4.9 %collective-permute-start.6 = (bf16[144,256]{1,0:T(8,128)(2,1)}, bf16[144,256]{1,0:T(8,128)(2,1)S(1)}, u32[]{:S(2)}, u32[]{:S(2)}) collective-permute-start(bf16[144,256]{1,0:T(8,128)(2,1)} %get-tuple-element.39), channel_id=1, source_target_pairs={{0,12},{1,13},{2,14},{3,15},{16,28},{17,29},{18,30},{19,31}} | collective-permute-start | bytes 221192 | tf_op jit(solution)/shard_map/ppermute | solution.py:34
  34.4 3.3 %collective-permute-start.5 = (bf16[144,256]{1,0:T(8,128)(2,1)}, bf16[144,256]{1,0:T(8,128)(2,1)S(1)}, u32[]{:S(2)}, u32[]{:S(2)}) collective-permute-start(bf16[144,256]{1,0:T(8,128)(2,1)} %get-tuple-element.39), channel_id=1, source_target_pairs={{0,8},{4,12},{1,9},{5,13},{2,10},{6,14},{3,11},{7,15},{16,24},{20,... | collective-permute-start | bytes 221192 | tf_op jit(solution)/shard_map/ppermute | solution.py:34
  37.7 1.3 %collective-permute-start.4 = (bf16[144,256]{1,0:T(8,128)(2,1)}, bf16[144,256]{1,0:T(8,128)(2,1)S(1)}, u32[]{:S(2)}, u32[]{:S(2)}) collective-permute-start(bf16[144,256]{1,0:T(8,128)(2,1)} %get-tuple-element.39), channel_id=1, source_target_pairs={{0,4},{4,8},{8,12},{1,5},{5,9},{9,13},{2,6},{6,10},{10,14},{3,7},{... | collective-permute-start | bytes 221192 | tf_op jit(solution)/shard_map/ppermute | solution.py:34
  39.0 0.7 constant_dynamic-update-slice_fusion.4
  39.7 0.8 pad_maximum_fusion.1
  40.5 1.5 %collective-permute-start.10 = (bf16[128,2176]{1,0:T(8,128)(2,1)}, bf16[128,2176]{1,0:T(8,128)(2,1)S(1)}, u32[]{:S(2)}, u32[]{:S(2)}) collective-permute-start(bf16[128,2176]{1,0:T(8,128)(2,1)} %pad_maximum_fusion.1), channel_id=1, source_target_pairs={{0,2},{1,3},{2,0},{3,1},{4,6},{5,7},{6,4},{7,5},{8,10},{9,11},{10,... | collective-permute-start | bytes 1671176 | tf_op jit(solution)/shard_map/ppermute | solution.py:28
  42.0 0.7 constant_dynamic-update-slice_fusion.3
  42.8 0.9 copy-done.6
  43.8 0.6 copy-done.3
  44.3 2.7 %gate.1 = (bf16[128,256]{1,0:T(8,128)(2,1)}, bf16[128,256]{1,0:T(8,128)(2,1)}, bf16[128,256]{1,0:T(8,128)(2,1)}, bf16[128,256]{1,0:T(8,128)(2,1)}) custom-call(f32[256,256]{1,0:T(8,128)} %inside.1.inside_ref, f32[256,128]{1,0:T(8,128)} %get-tuple-element.35.queries_ref, f32[256,256]{1,0:T(8,128)} %get-tuple-element.38.grown_ref, bf16[256,256]{1,0:T(8,128)(2,1)} %gate_ref.1, ...), custom_call_target="tpu_custom_call" | custom-call | tf_op jit(solution)/shard_map/gate/pallas_call | solution.py:377
  47.0 0.6 collective-permute-start.7
  47.7 3.1 %collective-permute-start.9 = (bf16[128,256]{1,0:T(8,128)(2,1)}, bf16[128,256]{1,0:T(8,128)(2,1)S(1)}, u32[]{:S(2)}, u32[]{:S(2)}) collective-permute-start(bf16[128,256]{1,0:T(8,128)(2,1)} %get-tuple-element.43), channel_id=1, source_target_pairs={{0,12},{4,0},{8,4},{12,8},{1,13},{5,1},{9,5},{13,9},{2,14},{6,2},{... | collective-permute-start | bytes 196616 | tf_op jit(solution)/shard_map/ppermute | solution.py:24
  50.8 0.7 constant_dynamic-update-slice_fusion.1
  51.5 1.9 %collective-permute-done.7 = bf16[128,256]{1,0:T(8,128)(2,1)S(1)} collective-permute-done((bf16[128,256]{1,0:T(8,128)(2,1)}, bf16[128,256]{1,0:T(8,128)(2,1)S(1)}, u32[]{:S(2)}, u32[]{:S(2)}) %collective-permute-start.7) | collective-permute-done | bytes 65568 | tf_op jit(solution)/shard_map/ppermute | solution.py:24
  53.4 1.2 %collective-permute-done.8 = bf16[128,256]{1,0:T(8,128)(2,1)S(1)} collective-permute-done((bf16[128,256]{1,0:T(8,128)(2,1)}, bf16[128,256]{1,0:T(8,128)(2,1)S(1)}, u32[]{:S(2)}, u32[]{:S(2)}) %collective-permute-start.8) | collective-permute-done | bytes 65568 | tf_op jit(solution)/shard_map/ppermute | solution.py:24
  54.7 0.9 pad_maximum_fusion.11
  55.6 1.2 %collective-permute-start.12 = (bf16[512,256]{1,0:T(8,128)(2,1)S(1)}, bf16[512,256]{1,0:T(8,128)(2,1)S(1)}, u32[]{:S(2)}, u32[]{:S(2)}) collective-permute-start(bf16[512,256]{1,0:T(8,128)(2,1)S(1)} %pad_maximum_fusion.5), channel_id=1, source_target_pairs={{0,2},{1,3},{2,0},{3,1},{4,6},{5,7},{6,4},{7,5},{8,10},{9,11},{10,... | collective-permute-start | bytes 786440 | tf_op jit(solution)/shard_map/ppermute | solution.py:28
  56.7 0.8 constant_dynamic-update-slice_fusion
  57.6 4.4 %collective-permute-done.12 = bf16[512,256]{1,0:T(8,128)(2,1)S(1)} collective-permute-done((bf16[512,256]{1,0:T(8,128)(2,1)S(1)}, bf16[512,256]{1,0:T(8,128)(2,1)S(1)}, u32[]{:S(2)}, u32[]{:S(2)}) %collective-permute-start.12) | collective-permute-done | bytes 262176 | tf_op jit(solution)/shard_map/ppermute | solution.py:28
  62.2 1.9 %collective-permute-done.13 = bf16[512,512]{1,0:T(8,128)(2,1)S(1)} collective-permute-done((bf16[512,512]{1,0:T(8,128)(2,1)S(1)}, bf16[512,512]{1,0:T(8,128)(2,1)S(1)}, u32[]{:S(2)}, u32[]{:S(2)}) %collective-permute-start.13) | collective-permute-done | bytes 524320 | tf_op jit(solution)/shard_map/ppermute | solution.py:28
  65.2 1.6 %copy-done.11 = bf16[1024,2048]{1,0:T(8,128)(2,1)S(1)} copy-done((bf16[1024,2048]{1,0:T(8,128)(2,1)S(1)}, bf16[1024,2048]{1,0:T(8,128)(2,1)}, u32[]{:S(2)}) %copy-start.11) | copy-done | bytes 4194328
  66.8 2.6 %multiply_reduce_fusion = (f32[512]{0:T(512)S(1)}, f32[512,2048]{1,0:T(8,128)S(1)}) fusion(bf16[1024,2048]{1,0:T(8,128)(2,1)S(1)} %copy-done.11, bf16[512,1024]{1,0:T(8,128)(2,1)S(1)} %dynamic-slice_dynamic-update-slice_fusion, f32[1024]{0:T(1024)S(1)} %copy-done.14, f32[512]{0:T(512)S(1)} %add_rsqrt_fusion.1, ...), kind=kOutput, calls=%fused_computation.1 | convolution fusion | flops 2155871744 | bytes 11542528 | tf_op jit(solution)/shard_map/dot_general | solution.py:419
  69.5 0.4 multiply_convert_fusion
  69.9 1.2 %copy-done.12 = bf16[2,2048,256]{2,1,0:T(8,128)(2,1)S(1)} copy-done((bf16[2,2048,256]{2,1,0:T(8,128)(2,1)S(1)}, bf16[2,2048,256]{2,1,0:T(8,128)(2,1)}, u32[]{:S(2)}) %copy-start.12) | copy-done | bytes 2097176
  71.0 0.8 fusion.13
  71.8 0.8 fusion.16
  72.6 0.4 select_reduce_fusion
  73.0 0.4 copy-done.13
  73.4 0.8 fusion.7
  74.2 0.8 fusion.6
  75.0 0.5 convolution_convert_fusion.5
  75.5 0.6 convolution_convert_fusion.4
  76.1 0.5 convolution_convert_fusion.3
  76.6 0.6 convolution_convert_fusion.2
  77.5 0.4 collective-permute-start.14
  78.1 0.5 fusion.46
  78.6 0.7 collective-permute-done.16
  79.3 0.6 add_convert_fusion.1
  79.8 1.2 %collective-permute-start.17 = (bf16[64,2048]{1,0:T(8,128)(2,1)S(1)}, bf16[64,2048]{1,0:T(8,128)(2,1)S(1)}, u32[]{:S(2)}, u32[]{:S(2)}) collective-permute-start(bf16[64,2048]{1,0:T(8,128)(2,1)S(1)} %add_convert_fusion.1), channel_id=1, source_target_pairs={{0,2},{1,3},{2,0},{3,1},{4,6},{5,7},{6,4},{7,5},{8,10},{9,11},{10,... | collective-permute-start | bytes 786440 | tf_op jit(solution)/shard_map/ppermute | solution.py:28
  81.0 0.6 add_convert_fusion.2
  81.6 1.0 collective-permute-start.15
  82.6 0.5 fusion.58
  83.1 6.0 %collective-permute-done.17 = bf16[64,2048]{1,0:T(8,128)(2,1)S(1)} collective-permute-done((bf16[64,2048]{1,0:T(8,128)(2,1)S(1)}, bf16[64,2048]{1,0:T(8,128)(2,1)S(1)}, u32[]{:S(2)}, u32[]{:S(2)}) %collective-permute-start.17) | collective-permute-done | bytes 262176 | tf_op jit(solution)/shard_map/ppermute | solution.py:28
  89.1 4.8 %collective-permute-done.15 = bf16[64,2048]{1,0:T(8,128)(2,1)S(1)} collective-permute-done((bf16[64,2048]{1,0:T(8,128)(2,1)S(1)}, bf16[64,2048]{1,0:T(8,128)(2,1)S(1)}, u32[]{:S(2)}, u32[]{:S(2)}) %collective-permute-start.15) | collective-permute-done | bytes 262176 | tf_op jit(solution)/shard_map/ppermute | solution.py:28
  94.2 2.5 %collective-permute-start.18 = (bf16[32,2048]{1,0:T(8,128)(2,1)S(1)}, bf16[32,2048]{1,0:T(8,128)(2,1)S(1)}, u32[]{:S(2)}, u32[]{:S(2)}) collective-permute-start(bf16[32,2048]{1,0:T(8,128)(2,1)S(1)} %get-tuple-element.70), channel_id=1, source_target_pairs={{0,12},{4,0},{8,4},{12,8},{1,13},{5,1},{9,5},{13,9},{2,14},{6,2},{... | collective-permute-start | bytes 393224 | tf_op jit(solution)/shard_map/ppermute | solution.py:24
  96.7 1.1 collective-permute-start.19
  97.9 2.7 %collective-permute-done.18 = bf16[32,2048]{1,0:T(8,128)(2,1)S(1)} collective-permute-done((bf16[32,2048]{1,0:T(8,128)(2,1)S(1)}, bf16[32,2048]{1,0:T(8,128)(2,1)S(1)}, u32[]{:S(2)}, u32[]{:S(2)}) %collective-permute-start.18) | collective-permute-done | bytes 131104 | tf_op jit(solution)/shard_map/ppermute | solution.py:24
  100.6 8.3 %collective-permute-done.19 = bf16[32,2048]{1,0:T(8,128)(2,1)S(1)} collective-permute-done((bf16[32,2048]{1,0:T(8,128)(2,1)S(1)}, bf16[32,2048]{1,0:T(8,128)(2,1)S(1)}, u32[]{:S(2)}, u32[]{:S(2)}) %collective-permute-start.19) | collective-permute-done | bytes 131104 | tf_op jit(solution)/shard_map/ppermute | solution.py:24
  108.9 1.0 convolution_convert_fusion.1
  (76 shorter events, 2.5 us)
Async XLA Ops:
  0.0 75.0 %copy-start = (bf16[2,256,2048]{2,1,0:T(8,128)(2,1)S(1)}, bf16[2,256,2048]{2,1,0:T(8,128)(2,1)}, u32[]{:S(2)}) copy-start(bf16[2,256,2048]{2,1,0:T(8,128)(2,1)} %param.36) | copy-start | bytes 6291460
  0.0 17.7 %copy-start.10 = (f32[4]{0:T(128)S(1)}, f32[4]{0:T(128)}, u32[]{:S(2)}) copy-start(f32[4]{0:T(128)} %param.27) | copy-start | bytes 52
  2.2 11.1 %copy-start.7 = (bf16[16,512]{1,0:T(8,128)(2,1)S(1)}, bf16[16,512]{1,0:T(8,128)(2,1)}, u32[]{:S(2)}) copy-start(bf16[16,512]{1,0:T(8,128)(2,1)} %tails.1) | copy-start | bytes 49156
  7.1 22.4 %collective-permute-start.3 = (bf16[32,2176]{1,0:T(8,128)(2,1)S(1)}, bf16[32,2176]{1,0:T(8,128)(2,1)S(1)}, u32[]{:S(2)}, u32[]{:S(2)}) collective-permute-start(bf16[32,2176]{1,0:T(8,128)(2,1)S(1)} %get-tuple-element.64), channel_id=1, source_target_pairs={{0,12},{4,0},{8,4},{12,8},{1,13},{5,1},{9,5},{13,9},{2,14},{6,2},{... | collective-permute-start | bytes 417800 | tf_op jit(solution)/shard_map/ppermute | solution.py:24
  12.2 17.3 %collective-permute-start.2 = (bf16[32,2176]{1,0:T(8,128)(2,1)S(1)}, bf16[32,2176]{1,0:T(8,128)(2,1)S(1)}, u32[]{:S(2)}, u32[]{:S(2)}) collective-permute-start(bf16[32,2176]{1,0:T(8,128)(2,1)S(1)} %get-tuple-element.65), channel_id=1, source_target_pairs={{0,8},{4,12},{8,0},{12,4},{1,9},{5,13},{9,1},{13,5},{2,10},{6,14},... | collective-permute-start | bytes 417800 | tf_op jit(solution)/shard_map/ppermute | solution.py:24
  12.2 17.3 %collective-permute-start.1 = (bf16[32,2176]{1,0:T(8,128)(2,1)S(1)}, bf16[32,2176]{1,0:T(8,128)(2,1)S(1)}, u32[]{:S(2)}, u32[]{:S(2)}) collective-permute-start(bf16[32,2176]{1,0:T(8,128)(2,1)S(1)} %get-tuple-element.66), channel_id=1, source_target_pairs={{0,4},{4,8},{8,12},{12,0},{1,5},{5,9},{9,13},{13,1},{2,6},{6,10},{... | collective-permute-start | bytes 417800 | tf_op jit(solution)/shard_map/ppermute | solution.py:24
  13.3 8.3 %collective-permute-start = (bf16[16,512]{1,0:T(8,128)(2,1)S(1)}, bf16[16,512]{1,0:T(8,128)(2,1)S(1)}, u32[]{:S(2)}, u32[]{:S(2)}) collective-permute-start(bf16[16,512]{1,0:T(8,128)(2,1)S(1)} %copy-done.7), channel_id=1, source_target_pairs={{0,4},{4,8},{8,12},{1,5},{5,9},{9,13},{2,6},{6,10},{10,14},{3,7},{... | collective-permute-start | bytes 49160 | tf_op jit(solution)/shard_map/ppermute | solution.py:34
  21.6 0.6 copy-start.8
  29.5 13.2 %collective-permute-start.6 = (bf16[144,256]{1,0:T(8,128)(2,1)}, bf16[144,256]{1,0:T(8,128)(2,1)S(1)}, u32[]{:S(2)}, u32[]{:S(2)}) collective-permute-start(bf16[144,256]{1,0:T(8,128)(2,1)} %get-tuple-element.39), channel_id=1, source_target_pairs={{0,12},{1,13},{2,14},{3,15},{16,28},{17,29},{18,30},{19,31}} | collective-permute-start | bytes 221192 | tf_op jit(solution)/shard_map/ppermute | solution.py:34
  34.4 8.3 %collective-permute-start.5 = (bf16[144,256]{1,0:T(8,128)(2,1)}, bf16[144,256]{1,0:T(8,128)(2,1)S(1)}, u32[]{:S(2)}, u32[]{:S(2)}) collective-permute-start(bf16[144,256]{1,0:T(8,128)(2,1)} %get-tuple-element.39), channel_id=1, source_target_pairs={{0,8},{4,12},{1,9},{5,13},{2,10},{6,14},{3,11},{7,15},{16,24},{20,... | collective-permute-start | bytes 221192 | tf_op jit(solution)/shard_map/ppermute | solution.py:34
  37.7 5.0 %collective-permute-start.4 = (bf16[144,256]{1,0:T(8,128)(2,1)}, bf16[144,256]{1,0:T(8,128)(2,1)S(1)}, u32[]{:S(2)}, u32[]{:S(2)}) collective-permute-start(bf16[144,256]{1,0:T(8,128)(2,1)} %get-tuple-element.39), channel_id=1, source_target_pairs={{0,4},{4,8},{8,12},{1,5},{5,9},{9,13},{2,6},{6,10},{10,14},{3,7},{... | collective-permute-start | bytes 221192 | tf_op jit(solution)/shard_map/ppermute | solution.py:34
  40.5 14.1 %collective-permute-start.10 = (bf16[128,2176]{1,0:T(8,128)(2,1)}, bf16[128,2176]{1,0:T(8,128)(2,1)S(1)}, u32[]{:S(2)}, u32[]{:S(2)}) collective-permute-start(bf16[128,2176]{1,0:T(8,128)(2,1)} %pad_maximum_fusion.1), channel_id=1, source_target_pairs={{0,2},{1,3},{2,0},{3,1},{4,6},{5,7},{6,4},{7,5},{8,10},{9,11},{10,... | collective-permute-start | bytes 1671176 | tf_op jit(solution)/shard_map/ppermute | solution.py:28
  42.7 1.0 copy-start.6
  42.7 1.0 copy-start.1
  42.8 1.0 copy-start.2
  43.7 0.6 copy-start.3
  47.0 15.1 %copy-start.4 = (bf16[512,2176]{1,0:T(8,128)(2,1)S(1)}, bf16[512,2176]{1,0:T(8,128)(2,1)}, u32[]{:S(2)}) copy-start(bf16[512,2176]{1,0:T(8,128)(2,1)} %get-tuple-element.73) | copy-start | bytes 6684676
  47.0 6.4 %collective-permute-start.7 = (bf16[128,256]{1,0:T(8,128)(2,1)}, bf16[128,256]{1,0:T(8,128)(2,1)S(1)}, u32[]{:S(2)}, u32[]{:S(2)}) collective-permute-start(bf16[128,256]{1,0:T(8,128)(2,1)} %get-tuple-element.41), channel_id=1, source_target_pairs={{0,4},{4,8},{8,12},{12,0},{1,5},{5,9},{9,13},{13,1},{2,6},{6,10},{... | collective-permute-start | bytes 196616 | tf_op jit(solution)/shard_map/ppermute | solution.py:24
  47.6 7.1 %collective-permute-start.8 = (bf16[128,256]{1,0:T(8,128)(2,1)}, bf16[128,256]{1,0:T(8,128)(2,1)S(1)}, u32[]{:S(2)}, u32[]{:S(2)}) collective-permute-start(bf16[128,256]{1,0:T(8,128)(2,1)} %get-tuple-element.42), channel_id=1, source_target_pairs={{0,8},{4,12},{8,0},{12,4},{1,9},{5,13},{9,1},{13,5},{2,10},{6,14},... | collective-permute-start | bytes 196616 | tf_op jit(solution)/shard_map/ppermute | solution.py:24
  47.7 6.9 %collective-permute-start.9 = (bf16[128,256]{1,0:T(8,128)(2,1)}, bf16[128,256]{1,0:T(8,128)(2,1)S(1)}, u32[]{:S(2)}, u32[]{:S(2)}) collective-permute-start(bf16[128,256]{1,0:T(8,128)(2,1)} %get-tuple-element.43), channel_id=1, source_target_pairs={{0,12},{4,0},{8,4},{12,8},{1,13},{5,1},{9,5},{13,9},{2,14},{6,2},{... | collective-permute-start | bytes 196616 | tf_op jit(solution)/shard_map/ppermute | solution.py:24
  55.6 6.4 %collective-permute-start.12 = (bf16[512,256]{1,0:T(8,128)(2,1)S(1)}, bf16[512,256]{1,0:T(8,128)(2,1)S(1)}, u32[]{:S(2)}, u32[]{:S(2)}) collective-permute-start(bf16[512,256]{1,0:T(8,128)(2,1)S(1)} %pad_maximum_fusion.5), channel_id=1, source_target_pairs={{0,2},{1,3},{2,0},{3,1},{4,6},{5,7},{6,4},{7,5},{8,10},{9,11},{10,... | collective-permute-start | bytes 786440 | tf_op jit(solution)/shard_map/ppermute | solution.py:28
  57.6 7.4 %collective-permute-start.11 = (bf16[256,2176]{1,0:T(8,128)(2,1)}, bf16[256,2176]{1,0:T(8,128)(2,1)S(1)}, u32[]{:S(2)}, u32[]{:S(2)}) collective-permute-start(bf16[256,2176]{1,0:T(8,128)(2,1)} %constant_dynamic-update-slice_fusion), channel_id=1, source_target_pairs={{0,1},{1,0},{2,3},{3,2},{4,5},{5,4},{6,7},{7,6},{8,9},{9,8},{10,11... | collective-permute-start | bytes 3342344 | tf_op jit(solution)/shard_map/ppermute | solution.py:28
  62.0 2.0 %collective-permute-start.13 = (bf16[512,512]{1,0:T(8,128)(2,1)S(1)}, bf16[512,512]{1,0:T(8,128)(2,1)S(1)}, u32[]{:S(2)}, u32[]{:S(2)}) collective-permute-start(bf16[512,512]{1,0:T(8,128)(2,1)S(1)} %pad_maximum_fusion.2), channel_id=1, source_target_pairs={{0,1},{1,0},{2,3},{3,2},{4,5},{5,4},{6,7},{7,6},{8,9},{9,8},{10,11... | collective-permute-start | bytes 1572872 | tf_op jit(solution)/shard_map/ppermute | solution.py:28
  64.6 2.2 %copy-start.11 = (bf16[1024,2048]{1,0:T(8,128)(2,1)S(1)}, bf16[1024,2048]{1,0:T(8,128)(2,1)}, u32[]{:S(2)}) copy-start(bf16[1024,2048]{1,0:T(8,128)(2,1)} %param.32) | copy-start | bytes 12582916
  64.9 1.9 %copy-start.14 = (f32[1024]{0:T(1024)S(1)}, f32[1024]{0:T(1024)}, u32[]{:S(2)}) copy-start(f32[1024]{0:T(1024)} %param.31) | copy-start | bytes 12292
  66.8 2.6 %copy-start.9 = (f32[2048]{0:T(1024)S(1)}, f32[2048]{0:T(1024)}, u32[]{:S(2)}) copy-start(f32[2048]{0:T(1024)} %param.33) | copy-start | bytes 24580
  69.5 1.6 %copy-start.12 = (bf16[2,2048,256]{2,1,0:T(8,128)(2,1)S(1)}, bf16[2,2048,256]{2,1,0:T(8,128)(2,1)}, u32[]{:S(2)}) copy-start(bf16[2,2048,256]{2,1,0:T(8,128)(2,1)} %param.34) | copy-start | bytes 6291460
  71.8 1.6 %copy-start.13 = (bf16[2,2048,256]{2,1,0:T(8,128)(2,1)S(1)}, bf16[2,2048,256]{2,1,0:T(8,128)(2,1)}, u32[]{:S(2)}) copy-start(bf16[2,2048,256]{2,1,0:T(8,128)(2,1)} %param.35) | copy-start | bytes 6291460
  77.3 2.0 %collective-permute-start.16 = (bf16[128,2048]{1,0:T(8,128)(2,1)S(1)}, bf16[128,2048]{1,0:T(8,128)(2,1)S(1)}, u32[]{:S(2)}, u32[]{:S(2)}) collective-permute-start(bf16[128,2048]{1,0:T(8,128)(2,1)S(1)} %pad_maximum_fusion.4), channel_id=1, source_target_pairs={{0,1},{1,0},{2,3},{3,2},{4,5},{5,4},{6,7},{7,6},{8,9},{9,8},{10,11... | collective-permute-start | bytes 1572872 | tf_op jit(solution)/shard_map/ppermute | solution.py:28
  77.5 3.5 %collective-permute-start.14 = (bf16[128,2048]{1,0:T(8,128)(2,1)S(1)}, bf16[128,2048]{1,0:T(8,128)(2,1)S(1)}, u32[]{:S(2)}, u32[]{:S(2)}) collective-permute-start(bf16[128,2048]{1,0:T(8,128)(2,1)S(1)} %pad_maximum_fusion.3), channel_id=1, source_target_pairs={{0,1},{1,0},{2,3},{3,2},{4,5},{5,4},{6,7},{7,6},{8,9},{9,8},{10,11... | collective-permute-start | bytes 1572872 | tf_op jit(solution)/shard_map/ppermute | solution.py:28
  79.8 9.2 %collective-permute-start.17 = (bf16[64,2048]{1,0:T(8,128)(2,1)S(1)}, bf16[64,2048]{1,0:T(8,128)(2,1)S(1)}, u32[]{:S(2)}, u32[]{:S(2)}) collective-permute-start(bf16[64,2048]{1,0:T(8,128)(2,1)S(1)} %add_convert_fusion.1), channel_id=1, source_target_pairs={{0,2},{1,3},{2,0},{3,1},{4,6},{5,7},{6,4},{7,5},{8,10},{9,11},{10,... | collective-permute-start | bytes 786440 | tf_op jit(solution)/shard_map/ppermute | solution.py:28
  81.6 12.3 %collective-permute-start.15 = (bf16[64,2048]{1,0:T(8,128)(2,1)S(1)}, bf16[64,2048]{1,0:T(8,128)(2,1)S(1)}, u32[]{:S(2)}, u32[]{:S(2)}) collective-permute-start(bf16[64,2048]{1,0:T(8,128)(2,1)S(1)} %add_convert_fusion.2), channel_id=1, source_target_pairs={{0,2},{1,3},{2,0},{3,1},{4,6},{5,7},{6,4},{7,5},{8,10},{9,11},{10,... | collective-permute-start | bytes 786440 | tf_op jit(solution)/shard_map/ppermute | solution.py:28
  93.9 15.0 %copy-start.5 = (bf16[128,64]{1,0:T(8,128)(2,1)S(1)}, bf16[128,64]{1,0:T(8,128)(2,1)}, u32[]{:S(2)}) copy-start(bf16[128,64]{1,0:T(8,128)(2,1)} %pick_rows.2) | copy-start | bytes 49156
  94.2 6.4 %collective-permute-start.18 = (bf16[32,2048]{1,0:T(8,128)(2,1)S(1)}, bf16[32,2048]{1,0:T(8,128)(2,1)S(1)}, u32[]{:S(2)}, u32[]{:S(2)}) collective-permute-start(bf16[32,2048]{1,0:T(8,128)(2,1)S(1)} %get-tuple-element.70), channel_id=1, source_target_pairs={{0,12},{4,0},{8,4},{12,8},{1,13},{5,1},{9,5},{13,9},{2,14},{6,2},{... | collective-permute-start | bytes 393224 | tf_op jit(solution)/shard_map/ppermute | solution.py:24
  96.7 12.2 %collective-permute-start.19 = (bf16[32,2048]{1,0:T(8,128)(2,1)S(1)}, bf16[32,2048]{1,0:T(8,128)(2,1)S(1)}, u32[]{:S(2)}, u32[]{:S(2)}) collective-permute-start(bf16[32,2048]{1,0:T(8,128)(2,1)S(1)} %get-tuple-element.71), channel_id=1, source_target_pairs={{0,8},{4,12},{8,0},{12,4},{1,9},{5,13},{9,1},{13,5},{2,10},{6,14},... | collective-permute-start | bytes 393224 | tf_op jit(solution)/shard_map/ppermute | solution.py:24
  97.8 11.1 %collective-permute-start.20 = (bf16[32,2048]{1,0:T(8,128)(2,1)S(1)}, bf16[32,2048]{1,0:T(8,128)(2,1)S(1)}, u32[]{:S(2)}, u32[]{:S(2)}) collective-permute-start(bf16[32,2048]{1,0:T(8,128)(2,1)S(1)} %get-tuple-element.69), channel_id=1, source_target_pairs={{0,4},{4,8},{8,12},{12,0},{1,5},{5,9},{9,13},{13,1},{2,6},{6,10},{... | collective-permute-start | bytes 393224 | tf_op jit(solution)/shard_map/ppermute | solution.py:24
